TPU v7x, 32 devices: a whole 2x2x4 slice. The times are simulated.
32 devices in a mesh: dp: 4 (over y, x), kv: 4 (over z), tp: 2 (over core).
Axes of the slice: x: 2, y: 2, z: 4, core: 2. Of those that a mesh axis runs over, the one named last changes fastest.
Arguments:
- tokens: bfloat16 [8192, 1024], P(('dp', 'kv')), parts along dimension 0, may hold values from -6 to 6
- chosen: int32 [128, 2, 16], P(('dp', 'kv'), 'tp'), parts along dimension 0, may hold values from 0 to 31, as said below
- w_query: bfloat16 [1024, 512], P(None, 'tp'), may hold values from -0.1875 to 0.1875
- w_key_summary: bfloat16 [1024, 128], replicated, may hold values from -0.1875 to 0.1875
- w_value_summary: bfloat16 [1024, 128], replicated, may hold values from -0.1875 to 0.1875
- w_key_chosen: bfloat16 [1024, 128], replicated, may hold values from -0.1875 to 0.1875
- w_value_chosen: bfloat16 [1024, 128], replicated, may hold values from -0.1875 to 0.1875
- squeeze_key_in: bfloat16 [2048, 64], replicated, may hold values from -0.125 to 0.125
- squeeze_key_out: bfloat16 [64, 64], replicated, may hold values from -0.75 to 0.75
- squeeze_value_in: bfloat16 [2048, 64], replicated, may hold values from -0.125 to 0.125
- squeeze_value_out: bfloat16 [64, 64], replicated, may hold values from -0.75 to 0.75
- w_gates: bfloat16 [1024, 16], replicated, may hold values from -0.1875 to 0.1875
- w_out: bfloat16 [512, 1024], replicated, may hold values from -0.25 to 0.25
- out_gain: float32 [1024], replicated, may hold values from 0.1 to 1.9
Outputs:
- attended: bfloat16 [8192, 1024], P(('dp', 'kv'), 'tp'), parts along dimension 0
There are 4 independent parts, one for each index of `dp`. A program takes and returns all parts, laid end to end along the dimension named above; an argument that names none is the same for every part. Nothing has to cross between parts.
Inputs may be any that keep to these rules, and one draw needn't show every extreme that they name: The 16 blocks chosen by each query block and group are different and include the query block's own block; listed blocks after the query block have all their keys masked. Over the 8 query blocks of one aligned span of 512 positions and one group, at most 4 different chosen blocks lie in any other aligned span, and in every draw some span and group reaches 4.
All inputs are finite; a program needn't handle non-finite values.
Results may differ from a plain program's by a relative error of at most 0.005.
Values may be sent and summed in bfloat16 or wider, within the bound.
A program may use at most 128 MiB of HBM per device.

v0:
```python
import jax
import jax.numpy as jnp
from jax import lax
from jax.sharding import PartitionSpec as P

HEAD = 64
CMP_STRIDE = 16
CMP_LEN = 32
SEL = 64
TOPK = 16
CAP = 4


EPS = 1e-06


def from_behind(x, axis, by):
    length = lax.axis_size(axis)
    pairs = [(i, i + by) for i in range(length) if 0 <= i + by < length]
    return lax.ppermute(x, axis, pairs)


def project(tokens, weight):
    return jnp.dot(tokens, weight, preferred_element_type=jnp.float32).astype(jnp.bfloat16)


def group_columns(weight, my_group, column_count):
    return lax.dynamic_slice_in_dim(weight, my_group * column_count, column_count, 1)


def squeeze_local(rows, following_rows, w_in, w_out):
    feature_width = rows.shape[1]
    block_count = rows.shape[0] // CMP_STRIDE
    extended = jnp.concatenate([rows, following_rows], axis=0).reshape(
        block_count + 1, CMP_STRIDE, feature_width
    )
    joined = jnp.concatenate([extended[:-1], extended[1:]], axis=1).reshape(
        block_count, CMP_LEN * feature_width
    )
    hidden = jax.nn.gelu(jnp.dot(joined, w_in, preferred_element_type=jnp.float32)).astype(
        jnp.bfloat16
    )
    return jnp.dot(hidden, w_out, preferred_element_type=jnp.float32).astype(jnp.bfloat16)


def finish(weighted, weight_sum):
    denom = jnp.where(weight_sum > 0, weight_sum, 1.0)
    return weighted / denom[..., None]


def summary_branch(queries, complete_lookup, value_all, positions, score_scale):
    tok_count, heads_here, feature_width = queries.shape
    query_rows = min(512, tok_count)
    summary_ends = jnp.arange(complete_lookup.shape[0]) * CMP_STRIDE + CMP_LEN - 1

    def attend(inputs):
        query_part, time_part = inputs
        scores = (
            jnp.einsum(
                "qrd,cd->qrc", query_part, complete_lookup, preferred_element_type=jnp.float32
            )
            * score_scale
        )
        visible = (summary_ends[None, :] <= time_part[:, None])[:, None, :]
        masked = jnp.where(visible, scores, -1e30)
        peak_score = jnp.max(masked, axis=-1, keepdims=True)
        weights = jnp.where(visible, jnp.exp(masked - peak_score), 0.0)
        weighted = jnp.einsum(
            "qrc,cd->qrd",
            weights.astype(jnp.bfloat16),
            value_all,
            preferred_element_type=jnp.float32,
        )
        return finish(weighted, jnp.sum(weights, axis=-1))

    result = lax.map(
        attend,
        (
            queries.reshape(tok_count // query_rows, query_rows, heads_here, feature_width),
            positions.reshape(tok_count // query_rows, query_rows),
        ),
    )
    return result.reshape(tok_count, heads_here, feature_width)


def pick_by_asking(queries, picked, key_pick, value_pick, positions, score_scale):
    tok_count, heads_here, feature_width = queries.shape
    blocks_here = tok_count // SEL
    devices = lax.axis_size("kv")
    my_index = lax.axis_index("kv")
    overall_segment_tally = devices * blocks_here
    owners = picked // blocks_here
    local_index = picked % blocks_here
    block_hits = picked[:, :, None] == jnp.arange(overall_segment_tally)[None, None, :]
    needed = jnp.any(block_hits, axis=(0, 1)).reshape(devices, blocks_here).astype(jnp.int32)
    needed = jnp.where(jnp.arange(devices)[:, None] == my_index, 0, needed)
    slot_index = jnp.cumsum(needed, axis=1) - 1
    filled = (needed[:, :, None] == 1) & (slot_index[:, :, None] == jnp.arange(CAP)[None, None, :])
    wanted = jnp.sum(jnp.where(filled, jnp.arange(blocks_here)[None, :, None], 0), axis=1).astype(
        jnp.int32
    )
    asked_for = lax.all_to_all(wanted, "kv", split_axis=0, concat_axis=0, tiled=True)
    key_blocks = key_pick.reshape(blocks_here, SEL, feature_width)
    value_blocks = value_pick.reshape(blocks_here, SEL, feature_width)
    sent_keys = key_blocks[asked_for]
    sent_values = value_blocks[asked_for]
    came_keys, came_values = (
        lax.all_to_all(sent_keys, "kv", split_axis=0, concat_axis=0, tiled=True),
        lax.all_to_all(sent_values, "kv", split_axis=0, concat_axis=0, tiled=True),
    )
    table_keys = jnp.concatenate(
        [came_keys.reshape(devices * CAP, SEL, feature_width), key_blocks], axis=0
    )
    table_values = jnp.concatenate(
        [came_values.reshape(devices * CAP, SEL, feature_width), value_blocks], axis=0
    )
    slot_of = jnp.sum(
        jnp.where(block_hits, slot_index.reshape(overall_segment_tally)[None, None, :], 0), axis=-1
    )
    table_index = jnp.where(owners == my_index, devices * CAP + local_index, owners * CAP + slot_of)
    keys_here = table_keys[table_index]
    values_here = table_values[table_index]
    key_places = picked[:, :, None] * SEL + jnp.arange(SEL)[None, None, :]
    blocks_per_map = min(512, tok_count) // SEL
    map_count = blocks_here // blocks_per_map

    def attend(inputs):
        query_part, time_part, key_part, value_part, place_part = inputs
        scores = (
            jnp.einsum("aqrd,aksd->aqrks", query_part, key_part, preferred_element_type=jnp.float32)
            * score_scale
        )
        visible = place_part[:, None, None, :, :] <= time_part[:, :, None, None, None]
        masked = jnp.where(visible, scores, -1e30)
        peak_score = jnp.max(masked, axis=(-2, -1), keepdims=True)
        weights = jnp.where(visible, jnp.exp(masked - peak_score), 0.0)
        weighted = jnp.einsum(
            "aqrks,aksd->aqrd",
            weights.astype(jnp.bfloat16),
            value_part,
            preferred_element_type=jnp.float32,
        )
        return finish(weighted, jnp.sum(weights, axis=(-2, -1)))

    shaped = (
        queries.reshape(map_count, blocks_per_map, SEL, heads_here, feature_width),
        positions.reshape(map_count, blocks_per_map, SEL),
        keys_here.reshape(map_count, blocks_per_map, TOPK, SEL, feature_width),
        values_here.reshape(map_count, blocks_per_map, TOPK, SEL, feature_width),
        key_places.reshape(map_count, blocks_per_map, TOPK, SEL),
    )
    result = lax.map(attend, shaped)
    return result.reshape(tok_count, heads_here, feature_width)


def local(
    tokens,
    chosen,
    w_query,
    w_key_summary,
    w_value_summary,
    w_key_chosen,
    w_value_chosen,
    squeeze_key_in,
    squeeze_key_out,
    squeeze_value_in,
    squeeze_value_out,
    w_gates,
    w_out,
    out_gain,
):
    tok_count = tokens.shape[0]
    my_group = lax.axis_index("tp")
    heads_here = w_query.shape[1] // HEAD
    score_scale = HEAD ** (-0.5)
    positions = lax.axis_index("kv") * tok_count + jnp.arange(tok_count)
    queries = project(tokens, w_query).reshape(tok_count, heads_here, HEAD)
    key_raw = project(tokens, group_columns(w_key_summary, my_group, HEAD))
    value_raw = project(tokens, group_columns(w_value_summary, my_group, HEAD))
    key_pick = project(tokens, group_columns(w_key_chosen, my_group, HEAD))
    value_pick = project(tokens, group_columns(w_value_chosen, my_group, HEAD))
    boundary = jnp.stack([key_raw[:CMP_STRIDE], value_raw[:CMP_STRIDE]])
    following_rows = from_behind(boundary, "kv", -1)
    key_sum = squeeze_local(key_raw, following_rows[0], squeeze_key_in, squeeze_key_out)
    value_sum = squeeze_local(value_raw, following_rows[1], squeeze_value_in, squeeze_value_out)
    complete_lookup, value_all = (
        lax.all_gather(key_sum, "kv", axis=0, tiled=True),
        lax.all_gather(value_sum, "kv", axis=0, tiled=True),
    )
    summary_out = summary_branch(queries, complete_lookup, value_all, positions, score_scale)
    picked = chosen[:, 0, :]
    chosen_out = pick_by_asking(queries, picked, key_pick, value_pick, positions, score_scale)
    gate_cols = lax.dynamic_slice_in_dim(w_gates, my_group * heads_here * 2, heads_here * 2, 1)
    gate_values = jax.nn.sigmoid(
        jnp.dot(tokens, gate_cols, preferred_element_type=jnp.float32)
    ).reshape(tok_count, heads_here, 2)
    mixed_heads = (gate_values[..., 0:1] * summary_out + gate_values[..., 1:2] * chosen_out).astype(
        jnp.bfloat16
    )
    mixed_heads = mixed_heads.reshape(tok_count, heads_here * HEAD)
    width_out = w_out.shape[1]
    half_width = width_out // lax.axis_size("tp")
    columns = lax.dynamic_slice_in_dim(w_out, my_group * half_width, half_width, 1)

    def add_heads(running, piece):
        weight_rows = lax.slice_in_dim(columns, 0, piece.shape[1], axis=0)
        return running + jnp.dot(piece, weight_rows, preferred_element_type=jnp.float32)

    projected = add_heads(
        jnp.zeros((tok_count, columns.shape[1]), jnp.float32),
        jax.tree.map(lambda a: lax.all_gather(a, "tp", axis=1, tiled=True), mixed_heads),
    )
    row_power = lax.psum(jnp.sum(projected * projected, axis=-1, keepdims=True), "tp")
    normed = projected * lax.rsqrt(row_power / width_out + EPS)
    gain_part = lax.dynamic_slice_in_dim(out_gain, my_group * half_width, half_width, 0)
    return (normed * gain_part).astype(jnp.bfloat16)


def solution(mesh):
    in_specs = (
        P(("dp", "kv"), None),
        P(("dp", "kv"), "tp", None),
        P(None, "tp"),
        P(),
        P(),
        P(),
        P(),
        P(),
        P(),
        P(),
        P(),
        P(),
        P(),
        P(),
    )
    out_specs = P(("dp", "kv"), "tp")
    return jax.shard_map(local, mesh=mesh, in_specs=in_specs, out_specs=out_specs, check_vma=False)
```

profile of v0, /device:TPU:19, one launch (start us, length us, event | category | flops | bytes accessed | tf_op | source)
XLA Modules:
  0.0 109.3 jit_solution(2942781952028998141)
XLA Ops:
  0.0 0.9 fusion.37
  2.0 4.6 %all-to-all-start = ((s32[4,1,4]{2,1,0:T(1,128)}), s32[4,1,4]{2,1,0:T(1,128)S(1)}, u32[]{:S(2)}, u32[]{:S(2)}) async-start(s32[4,1,4]{2,1,0:T(1,128)} %bitcast.20), calls=%async_computation | async-start | bytes 4096 | tf_op jit(solution)/shard_map/all_to_all | solution.py:102
  6.7 1.6 %fusion.15 = bf16[512,64]{0,1:T(8,128)(2,1)S(1)} fusion(bf16[512,1024]{1,0:T(8,128)(2,1)S(1)} %copy-done, bf16[1024,128]{1,0:T(8,128)(2,1)} %param.17, s32[]{:T(128)S(6)} %select_n.124), kind=kOutput, calls=%fused_computation.26 | convolution fusion | flops 67141632 | bytes 1376260 | tf_op jit(solution)/shard_map/dot_general | solution.py:24
  8.2 1.6 %fusion.16 = bf16[512,64]{0,1:T(8,128)(2,1)S(1)} fusion(bf16[512,1024]{1,0:T(8,128)(2,1)S(1)} %copy-done, bf16[1024,128]{1,0:T(8,128)(2,1)} %param.18, s32[]{:T(128)S(6)} %select_n.124), kind=kOutput, calls=%fused_computation.27 | convolution fusion | flops 67141632 | bytes 1376260 | tf_op jit(solution)/shard_map/dot_general | solution.py:24
  9.9 2.2 %collective-permute-start = (bf16[2,16,64]{1,2,0:T(8,128)(2,1)S(1)}, bf16[2,16,64]{1,2,0:T(8,128)(2,1)S(1)}, u32[]{:S(2)}, u32[]{:S(2)}) collective-permute-start(bf16[2,16,64]{1,2,0:T(8,128)(2,1)S(1)} %pad_maximum_fusion.6), channel_id=1, source_target_pairs={{2,0},{4,2},{6,4},{3,1},{5,3},{7,5},{10,8},{12,10},{14,12},{11,9},... | collective-permute-start | bytes 12296 | tf_op jit(solution)/shard_map/ppermute | solution.py:20
  13.1 1.6 %fusion.17 = bf16[512,64]{0,1:T(8,128)(2,1)S(1)} fusion(bf16[512,1024]{1,0:T(8,128)(2,1)S(1)} %copy-done, bf16[1024,128]{1,0:T(8,128)(2,1)} %param.19, s32[]{:T(128)S(6)} %select_n.124), kind=kOutput, calls=%fused_computation.28 | convolution fusion | flops 67141632 | bytes 1376260 | tf_op jit(solution)/shard_map/dot_general | solution.py:24
  14.8 1.0 select_reduce_fusion
  16.7 1.5 %convolution_convert_fusion = bf16[512,256]{0,1:T(8,128)(2,1)S(1)} fusion(bf16[512,1024]{1,0:T(8,128)(2,1)S(1)} %copy-done, bf16[1024,256]{1,0:T(8,128)(2,1)} %param.16), kind=kOutput, calls=%fused_computation.21 | convolution fusion | flops 268566528 | bytes 1835008 | tf_op jit(solution)/shard_map/dot_general | solution.py:24
  18.2 1.1 squeeze.34
  19.3 1.6 %fusion.18 = bf16[512,64]{0,1:T(8,128)(2,1)S(1)} fusion(bf16[512,1024]{1,0:T(8,128)(2,1)S(1)} %copy-done, bf16[1024,128]{1,0:T(8,128)(2,1)} %param.20, s32[]{:T(128)S(6)} %select_n.124), kind=kOutput, calls=%fused_computation.29 | convolution fusion | flops 67141632 | bytes 1376260 | tf_op jit(solution)/shard_map/dot_general | solution.py:24
  21.0 1.1 %fusion.22 = f32[512,8]{0,1:T(8,128)S(1)} fusion(bf16[512,1024]{1,0:T(8,128)(2,1)S(1)} %copy-done, bf16[1024,16]{0,1:T(8,128)(2,1)} %param.25, s32[]{:T(128)S(6)} %select_n.123), kind=kOutput, calls=%fused_computation.34 | convolution fusion | flops 8400896 | bytes 1081348 | tf_op jit(solution)/shard_map/dot_general | solution.py:195
  22.2 2.5 %broadcast_compare_fusion = pred[8,64,16,64]{1,3,2,0:T(8,128)(4,1)} fusion(s32[8,64]{1,0:T(8,128)S(1)} %add_add_fusion, s32[8,16,64]{2,1,0:T(8,128)S(1)} %iota_add_fusion), kind=kLoop, calls=%fused_computation.12 | loop fusion | flops 524288 | bytes 559104 | tf_op jit(solution)/shard_map/while/body/eval_jaxpr/le | solution.py:133
  26.3 0.9 reshape.366
  27.2 4.5 %all-to-all-start.1 = ((bf16[4,2,8192]{2,1,0:T(2,128)(2,1)}), bf16[4,2,8192]{2,1,0:T(2,128)(2,1)S(1)}, u32[]{:S(2)}, u32[]{:S(2)}) async-start(bf16[4,2,8192]{2,1,0:T(2,128)(2,1)} %reshape.366), calls=%async_computation.1 | async-start | bytes 262144 | tf_op jit(solution)/shard_map/all_to_all | solution.py:108
  32.3 0.9 reshape.364
  33.8 1.3 %convolution_convert_fusion.6 = bf16[32,64]{1,0:T(8,128)(2,1)S(1)} fusion(bf16[64,64]{1,0:T(8,128)(2,1)} %param.22, bf16[32,2048]{1,0:T(8,128)(2,1)S(1)} %reshape.314, bf16[2048,64]{0,1:T(8,128)(2,1)} %param.21), kind=kOutput, calls=%fused_computation.36 | convolution fusion | flops 8671232 | bytes 405504 | tf_op jit(solution)/shard_map/dot_general | solution.py:43
  35.1 8.4 %all_gather.9 = bf16[128,64]{1,0:T(8,128)(2,1)S(1)} all-gather(bf16[32,64]{1,0:T(8,128)(2,1)S(1)} %convolution_convert_fusion.6), channel_id=1, replica_groups=mesh['dp'=4,'kv'=4,'tp'=2] {'kv'}, dimensions={0}, use_global_device_ids=true | all-gather | bytes 20480 | tf_op jit(solution)/shard_map/all_gather | solution.py:187
  45.2 10.2 %all_gather.10 = bf16[128,64]{1,0:T(8,128)(2,1)S(1)} all-gather(bf16[32,64]{1,0:T(8,128)(2,1)S(1)} %convolution_convert_fusion.5), channel_id=1, replica_groups=mesh['dp'=4,'kv'=4,'tp'=2] {'kv'}, dimensions={0}, use_global_device_ids=true | all-gather | bytes 20480 | tf_op jit(solution)/shard_map/all_gather | solution.py:188
  55.4 1.2 %fusion.14 = f32[512,4,64]{0,2,1:T(8,128)} fusion(f32[512,4]{0,1:T(4,128)S(1)} %compare_select_fusion.1, f32[512,4]{0,1:T(4,128)S(1)} %get-tuple-element.60, f32[512,4,128]{0,2,1:T(8,128)S(1)} %fusion.13, pred[512,128]{0,1:T(8,128)(4,1)S(1)} %broadcast_compare_fusion.1, bf16[128,64]{1,0:T(8,128)(2,1)S(1)} %all_gather.10), kind=kOutput, calls=%fused_computation.20 | convolution fusion | flops 34605184 | bytes 1671168 | tf_op jit(solution)/shard_map/while/body/eval_jaxpr/qrc,cd->qrd/dot_general | solution.py:68
  56.6 6.3 %all-to-all-start.2 = ((bf16[4,2,8192]{2,1,0:T(2,128)(2,1)}), bf16[4,2,8192]{2,1,0:T(2,128)(2,1)}, u32[]{:S(2)}, u32[]{:S(2)}) async-start(bf16[4,2,8192]{2,1,0:T(2,128)(2,1)} %reshape.364), calls=%async_computation.2 | async-start | bytes 262144 | tf_op jit(solution)/shard_map/all_to_all | solution.py:109
  63.2 1.0 gather_fusion.1
  64.2 4.4 %fusion.1 = (f32[8,64,4]{1,2,0:T(4,128)S(1)}, f32[8,64,4,16,64]{1,4,3,2,0:T(8,128)S(1)}) fusion(pred[8,64,16,64]{1,3,2,0:T(8,128)(4,1)} %broadcast_compare_fusion, bf16[8,16,64,64,1]{3,2,1,4,0:T(8,128)(2,1)S(1)} %bitcast.111, bf16[8,64,4,64,1]{1,0,3,2,4:T(8,128)(2,1)} %bitcast.112), kind=kOutput, calls=%fused_computation.7 | convolution fusion | flops 274724864 | bytes 10231808 | tf_op jit(solution)/shard_map/while/body/eval_jaxpr/aqrd,aksd->aqrks/dot_general | solution.py:130
  68.6 6.0 %copy-done.1 = f32[8,64,4,16,64]{1,4,3,2,0:T(8,128)} copy-done((f32[8,64,4,16,64]{1,4,3,2,0:T(8,128)}, f32[8,64,4,16,64]{1,4,3,2,0:T(8,128)S(1)}, u32[]{:S(2)}) %copy-start.1) | copy-done | bytes 8388632
  74.6 4.7 %fusion.2 = f32[8,64,4]{1,2,0:T(4,128)S(1)} fusion(f32[8,64,4,16,64]{1,4,3,2,0:T(8,128)S(1)} %get-tuple-element.45, f32[8,64,4]{1,2,0:T(4,128)S(1)} %get-tuple-element.44, pred[8,64,16,64]{1,3,2,0:T(8,128)(4,1)S(1)} %copy-done.2), kind=kLoop, calls=%fused_computation.8 | loop fusion | flops 10483712 | bytes 8929280 | tf_op jit(solution)/shard_map/while/body/eval_jaxpr/reduce_sum | solution.py:143
  79.3 1.1 %reshape.365 = bf16[4,4,64,64]{3,2,1,0:T(8,128)(2,1)S(1)} reshape(bf16[4,2,8192]{2,1,0:T(2,128)(2,1)} %all-to-all-done.2) | data formatting | bytes 262144
  80.5 2.2 %gather_fusion.3 = bf16[128,64,64]{2,1,0:T(8,128)(2,1)} fusion(bf16[24,64,64]{2,1,0:T(8,128)(2,1)S(1)} %pad_maximum_fusion.1, s32[1024]{0:T(1024)S(1)} %pad_clamp_fusion), kind=kCustom, calls=%fused_computation.3 | custom fusion | bytes 2097664 | tf_op jit(solution)/shard_map/gather | solution.py:122
  82.7 9.2 %fusion.23 = f32[8,64,4,64]{3,1,2,0:T(8,128)S(1)} fusion(bf16[8,16,64,64,1]{3,2,1,4,0:T(8,128)(2,1)} %bitcast.115, f32[8,64,4,16,64]{1,4,3,2,0:T(8,128)} %copy-done.1, f32[8,64,4]{1,2,0:T(4,128)S(1)} %get-tuple-element.44, pred[8,64,16,64]{1,3,2,0:T(8,128)(4,1)S(1)} %copy-done.3, f32[8,64,4]{1,2,0:T(4,128)S(1)} %compare_select_fusion), kind=kOutput, calls=%fused_computation.39 | convolution fusion | flops 279052288 | bytes 10502144 | tf_op jit(solution)/shard_map/while/body/eval_jaxpr/aqrks,aksd->aqrd/dot_general | solution.py:137
  92.6 1.2 %fusion.29 = bf16[512,256]{0,1:T(8,128)(2,1)S(1)} fusion(f32[512,256]{0,1:T(8,128)S(1)} %reshape.320, f32[512,4,64]{0,2,1:T(8,128)} %fusion.14, f32[512,4]{0,1:T(4,128)S(1)} %get-tuple-element.58), kind=kLoop, calls=%fused_computation.44 | loop fusion | flops 393216 | bytes 1318912 | tf_op jit(solution)/shard_map/convert_element_type | solution.py:197
  93.7 10.3 %all_gather.11 = bf16[512,512]{0,1:T(8,128)(2,1)S(1)} all-gather(bf16[512,256]{0,1:T(8,128)(2,1)S(1)} %fusion.29), channel_id=1, replica_groups=mesh['dp'=4,'kv'=4,'tp'=2] {'tp'}, dimensions={1}, use_global_device_ids=true | all-gather | bytes 786432 | tf_op jit(solution)/shard_map/all_gather | solution.py:211
  104.1 1.5 %multiply_reduce_fusion = (f32[512]{0:T(512)S(1)}, f32[512,512]{0,1:T(8,128)S(1)}) fusion(bf16[512,512]{0,1:T(8,128)(2,1)S(1)} %all_gather.11, bf16[512,1024]{1,0:T(8,128)(2,1)} %param.26, s32[]{:T(128)S(6)} %select_n.139), kind=kOutput, calls=%fused_computation.38 | convolution fusion | flops 268959232 | bytes 2099204 | tf_op jit(solution)/shard_map/dot_general | solution.py:207
  105.6 2.5 %psum.7 = f32[512,1]{0,1:T(1,128)S(1)} all-reduce(f32[512,1]{0,1:T(1,128)S(1)} %bitcast.134), channel_id=1, replica_groups=mesh['dp'=4,'kv'=4,'tp'=2] {'tp'}, use_global_device_ids=true, to_apply=%region_9.10 | all-reduce | flops 512 | bytes 4096 | tf_op jit(solution)/shard_map/psum | solution.py:213
  108.3 1.0 copy.62
  (72 shorter events, 9.0 us)
Async XLA Ops:
  0.0 6.7 %copy-start = (bf16[512,1024]{1,0:T(8,128)(2,1)S(1)}, bf16[512,1024]{1,0:T(8,128)(2,1)}, u32[]{:S(2)}) copy-start(bf16[512,1024]{1,0:T(8,128)(2,1)} %param.14) | copy-start | bytes 3145732
  0.0 44.8 %copy-start.6 = (bf16[2048,64]{0,1:T(8,128)(2,1)S(1)}, bf16[2048,64]{0,1:T(8,128)(2,1)}, u32[]{:S(2)}) copy-start(bf16[2048,64]{0,1:T(8,128)(2,1)} %param.23) | copy-start | bytes 786436
  0.0 44.9 %copy-start.7 = (bf16[64,64]{1,0:T(8,128)(2,1)S(1)}, bf16[64,64]{1,0:T(8,128)(2,1)}, u32[]{:S(2)}) copy-start(bf16[64,64]{1,0:T(8,128)(2,1)} %param.24) | copy-start | bytes 24580
  2.0 23.5 %all-to-all-start = ((s32[4,1,4]{2,1,0:T(1,128)}), s32[4,1,4]{2,1,0:T(1,128)S(1)}, u32[]{:S(2)}, u32[]{:S(2)}) async-start(s32[4,1,4]{2,1,0:T(1,128)} %bitcast.20), calls=%async_computation | async-start | bytes 4096 | tf_op jit(solution)/shard_map/all_to_all | solution.py:102
  9.9 23.3 %collective-permute-start = (bf16[2,16,64]{1,2,0:T(8,128)(2,1)S(1)}, bf16[2,16,64]{1,2,0:T(8,128)(2,1)S(1)}, u32[]{:S(2)}, u32[]{:S(2)}) collective-permute-start(bf16[2,16,64]{1,2,0:T(8,128)(2,1)S(1)} %pad_maximum_fusion.6), channel_id=1, source_target_pairs={{2,0},{4,2},{6,4},{3,1},{5,3},{7,5},{10,8},{12,10},{14,12},{11,9},... | collective-permute-start | bytes 12296 | tf_op jit(solution)/shard_map/ppermute | solution.py:20
  21.0 42.1 %copy-start.4 = (bf16[512,64]{1,0:T(8,128)(2,1)}, bf16[512,64]{1,0:T(8,128)(2,1)S(1)}, u32[]{:S(2)}) copy-start(bf16[512,64]{1,0:T(8,128)(2,1)S(1)} %copy.72) | copy-start | bytes 196612
  27.2 29.4 %all-to-all-start.1 = ((bf16[4,2,8192]{2,1,0:T(2,128)(2,1)}), bf16[4,2,8192]{2,1,0:T(2,128)(2,1)S(1)}, u32[]{:S(2)}, u32[]{:S(2)}) async-start(bf16[4,2,8192]{2,1,0:T(2,128)(2,1)} %reshape.366), calls=%async_computation.1 | async-start | bytes 262144 | tf_op jit(solution)/shard_map/all_to_all | solution.py:108
  56.6 22.7 %all-to-all-start.2 = ((bf16[4,2,8192]{2,1,0:T(2,128)(2,1)}), bf16[4,2,8192]{2,1,0:T(2,128)(2,1)}, u32[]{:S(2)}, u32[]{:S(2)}) async-start(bf16[4,2,8192]{2,1,0:T(2,128)(2,1)} %reshape.364), calls=%async_computation.2 | async-start | bytes 262144 | tf_op jit(solution)/shard_map/all_to_all | solution.py:109
  64.2 10.4 %copy-start.2 = (pred[8,64,16,64]{1,3,2,0:T(8,128)(4,1)S(1)}, pred[8,64,16,64]{1,3,2,0:T(8,128)(4,1)}, u32[]{:S(2)}) copy-start(pred[8,64,16,64]{1,3,2,0:T(8,128)(4,1)} %broadcast_compare_fusion) | copy-start | bytes 1572868
  68.6 6.0 %copy-start.1 = (f32[8,64,4,16,64]{1,4,3,2,0:T(8,128)}, f32[8,64,4,16,64]{1,4,3,2,0:T(8,128)S(1)}, u32[]{:S(2)}) copy-start(f32[8,64,4,16,64]{1,4,3,2,0:T(8,128)S(1)} %get-tuple-element.45) | copy-start | bytes 25165828
  68.6 11.8 %copy-start.5 = (bf16[512,64]{1,0:T(8,128)(2,1)S(1)}, bf16[512,64]{1,0:T(8,128)(2,1)}, u32[]{:S(2)}) copy-start(bf16[512,64]{1,0:T(8,128)(2,1)} %copy-done.4) | copy-start | bytes 196612
  68.6 14.1 %copy-start.3 = (pred[8,64,16,64]{1,3,2,0:T(8,128)(4,1)S(1)}, pred[8,64,16,64]{1,3,2,0:T(8,128)(4,1)}, u32[]{:S(2)}) copy-start(pred[8,64,16,64]{1,3,2,0:T(8,128)(4,1)} %broadcast_compare_fusion) | copy-start | bytes 1572868
where the time goes:
time: 111 us; the launch traced here: 109 us
  blocking collectives  31.4 us (28%)
  matrix products  27.7 us (25%)
  local copies, waits for them, and re-layouts  18.6 us (17%)
  starting transfers between devices  17.7 us (16%)
  other arithmetic  13.5 us (12%)
    all_gather x1, blocking collectives, local(): lax.all_gather(a, 'tp', axis=1, tiled=True)  10.3 us
    all_gather x1, blocking collectives, local(): lax.all_gather(value_sum, 'kv', axis=0, tiled=True)  10.2 us
    dot_general x1, matrix products, attend(): jnp.einsum('aqrks,aksd->aqrd', weights.astype(jnp.bfloat16), value_part,...  9.21 us
    unnamed x21, local copies, waits for them, and re-layouts  9.13 us
    all_gather x1, blocking collectives, local(): lax.all_gather(key_sum, 'kv', axis=0, tiled=True)  8.37 us
    dot_general x5, matrix products, project(): jnp.dot(tokens, weight, preferred_element_type=jnp.float32)  7.8 us
    all_to_all x1, starting transfers between devices, pick_by_asking(): lax.all_to_all(sent_values, 'kv', split_axis=0, concat_axis=0, tiled=True)  6.33 us
    reduce_sum x1, other arithmetic, attend(): return finish(weighted, jnp.sum(weights, axis=(-2, -1)))  4.68 us
  transfers between devices with their start and end apart: 4, of which 0 were waited for; matrix products, arithmetic and copies ran while one was open for 32% of the time, Pallas kernels for 0%

commit v1 on v0

v1 whole, which is shorter than its diff:
```python
import functools

import jax
import jax.numpy as jnp
from jax import lax
from jax.experimental import pallas as pl
from jax.experimental.pallas import tpu as pltpu
from jax.sharding import PartitionSpec as P

HEAD = 64
CMP_STRIDE = 16
CMP_LEN = 32
SEL = 64
LANES = 128
EPS = 1e-06
NEG = -1e30
MESH = pl.DeviceIdType.MESH
F32 = jnp.float32
BF16 = jnp.bfloat16


def dot(a, b):
    return jnp.dot(a, b, preferred_element_type=F32)


def dot_t(a, b):
    return lax.dot_general(a, b, (((1,), (1,)), ((), ())), preferred_element_type=F32)


def swap(x):
    return pltpu.roll(x, HEAD, 1)


def low_lanes(shape):
    return lax.broadcasted_iota(jnp.int32, shape, 1) < HEAD


def kernel(
    spans,
    tokens_h,
    chosen_ref,
    wq_h,
    wks_h,
    wvs_h,
    wkc_h,
    wvc_h,
    ski_h,
    sko_h,
    svi_h,
    svo_h,
    wg_h,
    wo_h,
    gain_ref,
    out_ref,
    tokens,
    wq,
    wsum,
    wcho,
    ski,
    sko,
    svi,
    svo,
    wg,
    wo,
    raw,
    kv_all,
    pre_all,
    sum_kv,
    q_s,
    gates,
    bias,
    acc,
    m_s,
    l_s,
    mixed_own,
    mixed_other,
    in_sem,
    kv_send,
    kv_recv,
    pre_send,
    pre_recv,
    mix_send,
    mix_recv,
):
    me = lax.axis_index("kv")
    group = lax.axis_index("tp")
    first = group == 0
    rows, _ = tokens.shape
    blocks = rows // SEL
    cmp_rows = rows // CMP_STRIDE
    heads = wq.shape[1] // HEAD
    q_rows = heads * SEL

    loads = [
        pltpu.make_async_copy(src, dst, in_sem.at[i])
        for i, (src, dst) in enumerate(
            [
                (wks_h, wsum.at[:, pl.ds(0, LANES)]),
                (wvs_h, wsum.at[:, pl.ds(LANES, LANES)]),
                (wkc_h, wcho.at[:, pl.ds(0, LANES)]),
                (wvc_h, wcho.at[:, pl.ds(LANES, LANES)]),
                (tokens_h, tokens),
                (ski_h, ski),
                (svi_h, svi),
                (wq_h, wq),
                (wg_h, wg),
                (sko_h, sko),
                (svo_h, svo),
                (wo_h, wo),
            ]
        )
    ]
    for load in loads:
        load.start()

    barrier = pltpu.get_barrier_semaphore()

    def greet(step, carry):
        other = lax.rem(me + step, spans)
        pl.semaphore_signal(barrier, inc=1, device_id={"kv": other}, device_id_type=MESH)
        return carry

    lax.fori_loop(1, spans, greet, 0)
    pl.semaphore_signal(barrier, inc=1, device_id={"tp": 1 - group}, device_id_type=MESH)

    for load in loads[:5]:
        load.wait()
    low = low_lanes((rows, LANES))

    def pair(both):
        k2, v2 = both[:, :LANES], both[:, LANES:]
        k_side = jnp.where(first, k2, swap(k2))
        v_side = jnp.where(first, swap(v2), v2)
        return jnp.where(low, k_side, v_side)

    raw[...] = pair(dot(tokens[...], wsum[...]))
    kv_all[me] = pair(dot(tokens[...], wcho[...])).astype(BF16)

    for load in loads[5:7]:
        load.wait()
    low_c = low_lanes((cmp_rows, LANES))
    key_tiles, value_tiles = [], []
    for a in range(CMP_STRIDE // 2):
        even = raw[pl.ds(2 * a, cmp_rows, stride=CMP_STRIDE), :]
        odd = raw[pl.ds(2 * a + 1, cmp_rows, stride=CMP_STRIDE), :]
        key_tiles.append(jnp.where(low_c, even, swap(odd)).astype(BF16))
        value_tiles.append(jnp.where(low_c, swap(even), odd).astype(BF16))
    half = CMP_STRIDE * HEAD
    joined_k = jnp.concatenate(key_tiles, axis=1)
    joined_v = jnp.concatenate(value_tiles, axis=1)
    head_sum = jnp.concatenate(
        [dot(joined_k, ski[pl.ds(0, half), :]), dot(joined_v, svi[pl.ds(0, half), :])], axis=1
    )
    tail_sum = jnp.concatenate(
        [dot(joined_k, ski[pl.ds(half, half), :]), dot(joined_v, svi[pl.ds(half, half), :])], axis=1
    )
    row_c = lax.broadcasted_iota(jnp.int32, (cmp_rows, LANES), 0)
    shifted = jnp.where(row_c < cmp_rows - 1, pltpu.roll(tail_sum, cmp_rows - 1, 0), 0.0)
    pre_all[me, pl.ds(0, cmp_rows), :] = head_sum + shifted
    pre_all[me, pl.ds(cmp_rows, 8), :] = tail_sum[:8]

    def clear(span, carry):
        pre_all[span] = jnp.zeros(pre_all.shape[1:], F32)
        return carry

    lax.fori_loop(me + 1, spans, clear, 0)

    pl.semaphore_wait(barrier, spans)

    def pre_copy(source, target):
        return pltpu.make_async_remote_copy(
            src_ref=pre_all.at[source],
            dst_ref=pre_all.at[source],
            send_sem=pre_send.at[target],
            recv_sem=pre_recv.at[source],
            device_id={"kv": target},
            device_id_type=MESH,
        )

    def kv_copy(source, target):
        return pltpu.make_async_remote_copy(
            src_ref=kv_all.at[source],
            dst_ref=kv_all.at[source],
            send_sem=kv_send.at[target],
            recv_sem=kv_recv.at[source],
            device_id={"kv": target},
            device_id_type=MESH,
        )

    def send_pre(step, carry):
        pre_copy(me, spans - 1 - step).start()
        return carry

    def send_kv(step, carry):
        kv_copy(me, spans - 1 - step).start()
        return carry

    lax.fori_loop(0, spans - 1 - me, send_pre, 0)
    lax.fori_loop(0, spans - 1 - me, send_kv, 0)

    for load in loads[7:9]:
        load.wait()
    scaled = dot(tokens[...], wq[...]).astype(BF16).astype(F32) * (HEAD**-0.5)
    for a in range(heads // 2):
        tile = scaled[:, a * LANES : (a + 1) * LANES]
        even = jnp.where(low, tile, 0.0).astype(BF16)
        odd = jnp.where(low, swap(tile), 0.0).astype(BF16)
        q_s[:, pl.ds(2 * a * SEL, SEL), :] = even.reshape(blocks, SEL, LANES)
        q_s[:, pl.ds((2 * a + 1) * SEL, SEL), :] = odd.reshape(blocks, SEL, LANES)
    gate_all = jax.nn.sigmoid(dot(tokens[...], wg[...]))
    width = 2 * heads
    gates[...] = jnp.where(first, gate_all[:, :width], gate_all[:, width : 2 * width])

    def set_bias(span):
        ids = span * blocks + lax.broadcasted_iota(jnp.int32, (blocks, rows), 1) // SEL
        picks = chosen_ref[:, 0, :]
        hit = jnp.zeros((blocks, rows), F32)
        for t in range(picks.shape[1]):
            hit = jnp.where(picks[:, t : t + 1] == ids, 1.0, hit)
        bias[...] = jnp.where(hit > 0.0, 0.0, NEG)

    def lane_sum(p):
        total = p[:, :LANES]
        for c in range(1, p.shape[1] // LANES):
            total = total + p[:, c * LANES : (c + 1) * LANES]
        return total

    set_bias(me)

    def own_block(j, carry):
        keys = kv_all[me]
        scores = dot_t(q_s[j], keys) + bias[pl.ds(j, 1), :]
        place = lax.broadcasted_iota(jnp.int32, scores.shape, 1)
        time = j * SEL + lax.broadcasted_iota(jnp.int32, scores.shape, 0) % SEL
        scores = jnp.where(place <= time, scores, NEG)
        peak = jnp.max(scores, axis=1, keepdims=True)
        p = jnp.exp(scores - peak)
        m_s[j] = jnp.broadcast_to(peak, (q_rows, LANES))
        l_s[j] = lane_sum(p)
        acc[j] = dot(p.astype(BF16), keys)
        return carry

    lax.fori_loop(0, blocks, own_block, 0)

    def span_step(step, carry):
        span = me - 1 - step
        set_bias(span)
        kv_copy(span, me).wait_recv()

        def block(j, inner):
            keys = kv_all[span]
            scores = dot_t(q_s[j], keys) + bias[pl.ds(j, 1), :]
            old = m_s[j]
            peak = jnp.maximum(old, jnp.max(scores, axis=1, keepdims=True))
            p = jnp.exp(scores - peak[:, :1])
            fix = jnp.exp(old - peak)
            m_s[j] = peak
            l_s[j] = l_s[j] * fix + lane_sum(p)
            acc[j] = acc[j] * fix + dot(p.astype(BF16), keys)
            return inner

        return lax.fori_loop(0, blocks, block, carry)

    lax.fori_loop(0, me, span_step, 0)

    def await_pre(span, carry):
        pre_copy(span, me).wait_recv()
        return carry

    lax.fori_loop(0, me, await_pre, 0)
    for load in loads[9:11]:
        load.wait()
    parts = []
    for span in range(spans):
        part = pre_all[span, pl.ds(0, cmp_rows), :]
        if span + 1 < spans:
            part = part + jnp.where(
                row_c == cmp_rows - 1, pre_all[span + 1, pl.ds(cmp_rows, 1), :], 0.0
            )
        parts.append(part)
    hidden = jax.nn.gelu(jnp.concatenate(parts, axis=0)).astype(BF16)
    sum_kv[...] = jnp.concatenate(
        [dot(hidden[:, :HEAD], sko[...]), dot(hidden[:, HEAD:], svo[...])], axis=1
    ).astype(BF16)

    low_q = low_lanes((SEL, LANES))

    def mix_copy(j):
        part = pl.ds(pl.multiple_of(j * SEL, SEL), SEL)
        return pltpu.make_async_remote_copy(
            src_ref=mixed_own.at[part, :],
            dst_ref=mixed_other.at[part, :],
            send_sem=mix_send.at[j],
            recv_sem=mix_recv.at[j],
            device_id={"tp": 1 - group},
            device_id_type=MESH,
        )

    def finish_block(j, carry):
        table = sum_kv[...]
        scores = dot_t(q_s[j], table)
        ends = lax.broadcasted_iota(jnp.int32, scores.shape, 1) * CMP_STRIDE + CMP_LEN - 1
        time = me * rows + j * SEL + lax.broadcasted_iota(jnp.int32, scores.shape, 0) % SEL
        visible = ends <= time
        scores = jnp.where(visible, scores, NEG)
        peak = jnp.max(scores, axis=1, keepdims=True)
        p = jnp.where(visible, jnp.exp(scores - peak), 0.0)
        weight = jnp.sum(p, axis=1, keepdims=True)
        summary = dot(p.astype(BF16), table) / jnp.where(weight > 0.0, weight, 1.0)
        picked = acc[j] / jnp.sum(l_s[j], axis=1, keepdims=True)
        part = pl.ds(pl.multiple_of(j * SEL, SEL), SEL)
        gate = gates[part, :]
        heads_out = []
        for h in range(heads):
            cut = slice(h * SEL, (h + 1) * SEL)
            heads_out.append(
                gate[:, 2 * h : 2 * h + 1] * summary[cut] + gate[:, 2 * h + 1 : 2 * h + 2] * picked[cut]
            )
        tiles = [
            jnp.where(low_q, swap(heads_out[2 * a]), heads_out[2 * a + 1]) for a in range(heads // 2)
        ]
        mixed_own[part, :] = jnp.concatenate(tiles, axis=1).astype(BF16)
        mix_copy(j).start()
        return carry

    lax.fori_loop(0, blocks, finish_block, 0)
    loads[11].wait()

    half_rows = heads * HEAD
    half_cols = wo.shape[1] // 2
    own_rows = pl.ds(pl.multiple_of(group * half_rows, half_rows), half_rows)
    other_rows = pl.ds(pl.multiple_of((1 - group) * half_rows, half_rows), half_rows)
    own_cols = pl.ds(pl.multiple_of(group * half_cols, half_cols), half_cols)
    other_cols = pl.ds(pl.multiple_of((1 - group) * half_cols, half_cols), half_cols)

    def project_block(j, carry):
        for b in range(2):
            mix_copy(2 * j + b).wait_recv()
        part = pl.ds(pl.multiple_of(2 * j * SEL, 2 * SEL), 2 * SEL)
        own, other = mixed_own[part, :], mixed_other[part, :]
        mine = dot(own, wo[own_rows, own_cols]) + dot(other, wo[other_rows, own_cols])
        rest = dot(own, wo[own_rows, other_cols]) + dot(other, wo[other_rows, other_cols])
        power = jnp.sum(mine * mine + rest * rest, axis=1, keepdims=True)
        scale = lax.rsqrt(power / wo.shape[1] + EPS)
        out_ref[part, :] = (mine * scale * gain_ref[:, own_cols]).astype(BF16)
        return carry

    lax.fori_loop(0, blocks // 2, project_block, 0)

    def end_mix(j, carry):
        mix_copy(j).wait_send()
        return carry

    lax.fori_loop(0, blocks, end_mix, 0)

    def end_sends(step, carry):
        pre_copy(me, spans - 1 - step).wait_send()
        kv_copy(me, spans - 1 - step).wait_send()
        return carry

    lax.fori_loop(0, spans - 1 - me, end_sends, 0)


def local(spans, tokens, chosen, *weights):
    w_query, w_ks, w_vs, w_kc, w_vc, ski, sko, svi, svo, w_gates, w_out, gain = weights
    rows, width = tokens.shape
    heads = w_query.shape[1] // HEAD
    blocks = rows // SEL
    cmp_rows = rows // CMP_STRIDE
    any_spec = pl.BlockSpec(memory_space=pl.ANY)
    vmem = pl.BlockSpec(memory_space=pltpu.VMEM)
    dma = pltpu.SemaphoreType.DMA
    return pl.pallas_call(
        functools.partial(kernel, spans),
        out_shape=jax.ShapeDtypeStruct((rows, w_out.shape[1] // 2), BF16),
        in_specs=[any_spec, vmem] + [any_spec] * 11 + [vmem],
        out_specs=vmem,
        scratch_shapes=[
            pltpu.VMEM(tokens.shape, BF16),
            pltpu.VMEM(w_query.shape, BF16),
            pltpu.VMEM((width, 2 * w_ks.shape[1]), BF16),
            pltpu.VMEM((width, 2 * w_kc.shape[1]), BF16),
            pltpu.VMEM(ski.shape, BF16),
            pltpu.VMEM(sko.shape, BF16),
            pltpu.VMEM(svi.shape, BF16),
            pltpu.VMEM(svo.shape, BF16),
            pltpu.VMEM(w_gates.shape, BF16),
            pltpu.VMEM(w_out.shape, BF16),
            pltpu.VMEM((rows, LANES), F32),
            pltpu.VMEM((spans, rows, LANES), BF16),
            pltpu.VMEM((spans, cmp_rows + 8, LANES), F32),
            pltpu.VMEM((spans * cmp_rows, LANES), BF16),
            pltpu.VMEM((blocks, heads * SEL, LANES), BF16),
            pltpu.VMEM((rows, 2 * heads), F32),
            pltpu.VMEM((blocks, rows), F32),
            pltpu.VMEM((blocks, heads * SEL, LANES), F32),
            pltpu.VMEM((blocks, heads * SEL, LANES), F32),
            pltpu.VMEM((blocks, heads * SEL, LANES), F32),
            pltpu.VMEM((rows, heads * HEAD), BF16),
            pltpu.VMEM((rows, heads * HEAD), BF16),
            dma((12,)),
            dma((spans,)),
            dma((spans,)),
            dma((spans,)),
            dma((spans,)),
            dma((blocks,)),
            dma((blocks,)),
        ],
        compiler_params=pltpu.CompilerParams(collective_id=0, has_side_effects=True),
    )(
        tokens,
        chosen,
        w_query,
        w_ks,
        w_vs,
        w_kc,
        w_vc,
        ski,
        sko,
        svi,
        svo,
        w_gates,
        w_out,
        gain.reshape(1, -1),
    )


def solution(mesh):
    in_specs = (
        P(("dp", "kv"), None),
        P(("dp", "kv"), "tp", None),
        P(None, "tp"),
    ) + (P(),) * 11
    return jax.shard_map(
        functools.partial(local, mesh.shape["kv"]),
        mesh=mesh,
        in_specs=in_specs,
        out_specs=P(("dp", "kv"), "tp"),
        check_vma=False,
    )
```

time: 111 us -> 39.9 us (0.36); the launches traced: 109 us -> 39.7 us
  Pallas kernels: 0 us -> 34.2 us
  blocking collectives: 31.4 us -> 0 us
  matrix products: 27.7 us -> 0 us
  starting transfers between devices: 17.7 us -> 0 us
  other arithmetic: 13.5 us -> 0 us
  local copies, waits for them, and re-layouts: 18.6 us -> 5.53 us
    pallas_call x0 -> x1, Pallas kernels: none -> 34.2 us  [local(): pl.pallas_call(functools.partial(kernel, spans), out_shape=jax.ShapeDtype...]
    all_gather x3 -> x0, blocking collectives: 28.9 us -> none  [the longest x1 10.3 us: local(): lax.all_gather(a, 'tp', axis=1, tiled=True)]
    dot_general x13 -> x0, matrix products: 27.2 us -> none  [the longest x1 9.21 us: attend(): jnp.einsum('aqrks,aksd->aqrd', weights.astype(jnp.bfloat16), value_part,...]
    all_to_all x3 -> x0, starting transfers between devices: 15.5 us -> none  [the longest x1 6.33 us: pick_by_asking(): lax.all_to_all(sent_values, 'kv', split_axis=0, concat_axis=0, tiled=True)]
    reduce_sum x3 -> x0, other arithmetic: 6.41 us -> none  [the longest x1 4.68 us: attend(): return finish(weighted, jnp.sum(weights, axis=(-2, -1)))]
    gather x4 -> x0, local copies, waits for them, and re-layouts: 4.31 us -> none  [the longest x1 2.17 us: pick_by_asking(): values_here = table_values[table_index]]
    unnamed x21 -> x8, local copies, waits for them, and re-layouts: 9.13 us -> 5.53 us
    le x2 -> x0, other arithmetic: 2.58 us -> none  [the longest x1 2.48 us: attend(): place_part[:, None, None, :, :] <= time_part[:, :, None, None, None]]
  transfers between devices with their start and end apart: 4 -> 0, of which waited for: 0 -> 0; matrix products, arithmetic and copies ran while one was open for 32% -> 0% of each run, Pallas kernels for 0% -> 0%
where the time goes in v1:
time: 39.9 us; the launch traced here: 39.7 us
  Pallas kernels  34.2 us (86%)
  local copies, waits for them, and re-layouts  5.53 us (14%)
    pallas_call x1, Pallas kernels, local(): pl.pallas_call(functools.partial(kernel, spans), out_shape=jax.ShapeDtype...  34.2 us
    unnamed x8, local copies, waits for them, and re-layouts  5.53 us

profile of v1, /device:TPU:19, one launch (start us, length us, event | category | flops | bytes accessed | tf_op | source)
XLA Modules:
  0.0 39.7 jit_solution(14804496419339145325)
XLA Ops:
  0.0 0.0 copy-start
  0.0 1.7 %copy.17.wg_h = bf16[1024,16]{1,0:T(8,128)(2,1)} copy(bf16[1024,16]{0,1:T(8,128)(2,1)} %param.25) | data formatting | bytes 65536 | tf_op args[11]
  1.7 0.0 copy-done
  1.7 0.0 copy-start.1
  1.7 1.0 %copy.15.ski_h = bf16[2048,64]{1,0:T(8,128)(2,1)} copy(bf16[2048,64]{0,1:T(8,128)(2,1)S(1)} %copy-done) | data formatting | bytes 524288 | tf_op args[7]
  2.7 0.0 copy-done.1
  2.7 1.0 %copy.16.svi_h = bf16[2048,64]{1,0:T(8,128)(2,1)} copy(bf16[2048,64]{0,1:T(8,128)(2,1)S(1)} %copy-done.1) | data formatting | bytes 524288 | tf_op args[9]
  3.7 34.2 %shard_map.136 = bf16[512,512]{1,0:T(8,128)(2,1)} custom-call(bf16[512,1024]{1,0:T(8,128)(2,1)} %tokens_h.1, s32[8,1,16]{2,1,0:T(1,128)} %chosen_ref.1, bf16[1024,256]{1,0:T(8,128)(2,1)} %wq_h.1, bf16[1024,128]{1,0:T(8,128)(2,1)} %wks_h.1, bf16[1024,128]{1,0:T(8,128)(2,1)} %wvs_h.1, bf16[1024,128]{1,0:T(8,128)(2,1)} %wkc_h.1, bf16[1024,128]{1,0:T(8,128)(2,1)} %wvc_h.1, ...), custom_call_target="tpu_custom_call" | custom-call | tf_op jit(solution)/shard_map/pallas_call | solution.py:373
  37.8 1.9 %copy.19 = bf16[512,512]{1,0:T(8,128)(2,1)} copy(bf16[512,512]{1,0:T(8,128)(2,1)} %shard_map.136) | data formatting | bytes 1048576
Async XLA Ops:
  0.0 1.7 %copy-start = (bf16[2048,64]{0,1:T(8,128)(2,1)S(1)}, bf16[2048,64]{0,1:T(8,128)(2,1)}, u32[]{:S(2)}) copy-start(bf16[2048,64]{0,1:T(8,128)(2,1)} %param.21) | copy-start | bytes 786436
  1.7 1.0 %copy-start.1 = (bf16[2048,64]{0,1:T(8,128)(2,1)S(1)}, bf16[2048,64]{0,1:T(8,128)(2,1)}, u32[]{:S(2)}) copy-start(bf16[2048,64]{0,1:T(8,128)(2,1)} %param.23) | copy-start | bytes 786436

commit v2 on v1

--- a/solution.py
+++ b/solution.py
@@ -11,6 +11,7 @@
 CMP_STRIDE = 16
 CMP_LEN = 32
 SEL = 64
+CAP = 4
 LANES = 128
 EPS = 1e-06
 NEG = -1e30
@@ -63,18 +64,25 @@
     wg,
     wo,
     raw,
+    kv_own,
     kv_all,
+    packed,
+    asks,
+    slots,
     pre_all,
     sum_kv,
     q_s,
     gates,
     bias,
+    far_bias,
     acc,
     m_s,
     l_s,
     mixed_own,
     mixed_other,
     in_sem,
+    ask_send,
+    ask_recv,
     kv_send,
     kv_recv,
     pre_send,
@@ -95,11 +103,11 @@
         pltpu.make_async_copy(src, dst, in_sem.at[i])
         for i, (src, dst) in enumerate(
             [
-                (wks_h, wsum.at[:, pl.ds(0, LANES)]),
-                (wvs_h, wsum.at[:, pl.ds(LANES, LANES)]),
                 (wkc_h, wcho.at[:, pl.ds(0, LANES)]),
                 (wvc_h, wcho.at[:, pl.ds(LANES, LANES)]),
                 (tokens_h, tokens),
+                (wks_h, wsum.at[:, pl.ds(0, LANES)]),
+                (wvs_h, wsum.at[:, pl.ds(LANES, LANES)]),
                 (ski_h, ski),
                 (svi_h, svi),
                 (wq_h, wq),
@@ -123,9 +131,52 @@
     lax.fori_loop(1, spans, greet, 0)
     pl.semaphore_signal(barrier, inc=1, device_id={"tp": 1 - group}, device_id_type=MESH)
 
-    for load in loads[:5]:
-        load.wait()
     low = low_lanes((rows, LANES))
+
+    def ask_copy(source, target):
+        return pltpu.make_async_remote_copy(
+            src_ref=chosen_ref,
+            dst_ref=asks.at[source],
+            send_sem=ask_send.at[target],
+            recv_sem=ask_recv.at[source],
+            device_id={"kv": target},
+            device_id_type=MESH,
+        )
+
+    def kv_copy(source, target):
+        return pltpu.make_async_remote_copy(
+            src_ref=packed.at[target],
+            dst_ref=kv_all.at[source],
+            send_sem=kv_send.at[target],
+            recv_sem=kv_recv.at[source],
+            device_id={"kv": target},
+            device_id_type=MESH,
+        )
+
+    pl.semaphore_wait(barrier, spans)
+
+    def send_ask(span, carry):
+        ask_copy(me, span).start()
+        return carry
+
+    lax.fori_loop(0, me, send_ask, 0)
+
+    def block_of_slot(picks):
+        lanes = -(-spans * blocks // LANES) * LANES
+        ids = lax.broadcasted_iota(jnp.int32, (blocks, lanes), 1)
+        hit = jnp.zeros((blocks, lanes), jnp.int32)
+        for t in range(picks.shape[1]):
+            hit = jnp.where(picks[:, t : t + 1] == ids, 1, hit)
+        need = jnp.broadcast_to(jnp.max(hit, axis=0, keepdims=True), (8, lanes))
+        lane = lax.broadcasted_iota(jnp.int32, (8, lanes), 1)
+        rank = jnp.zeros((8, lanes), jnp.int32)
+        for d in range(1, blocks):
+            rank = rank + jnp.where(lane % blocks >= d, pltpu.roll(need, d, 1), 0)
+        code = jnp.where((need > 0) & (rank < CAP), lane // blocks * CAP + rank, -1)[:1]
+        place = lax.broadcasted_iota(jnp.int32, (spans * CAP, lanes), 0)
+        id_row = lax.broadcasted_iota(jnp.int32, (spans * CAP, lanes), 1)
+        found = jnp.where(code == place, id_row, -1)
+        return jnp.broadcast_to(jnp.max(found, axis=1, keepdims=True), (spans * CAP, LANES))
 
     def pair(both):
         k2, v2 = both[:, :LANES], both[:, LANES:]
@@ -133,8 +184,30 @@
         v_side = jnp.where(first, swap(v2), v2)
         return jnp.where(low, k_side, v_side)
 
+    for load in loads[:3]:
+        load.wait()
+    kv_own[...] = pair(dot(tokens[...], wcho[...])).astype(BF16)
+
+    def serve(step, carry):
+        target = spans - 1 - step
+        ask_copy(target, me).wait_recv()
+        slots[...] = block_of_slot(asks[target][:, 0, :])
+        key_lane = lax.broadcasted_iota(jnp.int32, (SEL, rows), 1)
+        key_row = lax.broadcasted_iota(jnp.int32, (SEL, rows), 0)
+        ours = slots[pl.ds(me * CAP, CAP), :]
+        pieces = []
+        for k in range(CAP):
+            start = (ours[k : k + 1, :1] - me * blocks) * SEL
+            pieces.append(jnp.where(key_lane == start + key_row, 1.0, 0.0).astype(BF16))
+        packed[target] = dot(jnp.concatenate(pieces, axis=0), kv_own[...]).astype(BF16)
+        kv_copy(me, target).start()
+        return carry
+
+    lax.fori_loop(0, spans - 1 - me, serve, 0)
+
+    for load in loads[3:5]:
+        load.wait()
     raw[...] = pair(dot(tokens[...], wsum[...]))
-    kv_all[me] = pair(dot(tokens[...], wcho[...])).astype(BF16)
 
     for load in loads[5:7]:
         load.wait()
@@ -149,10 +222,10 @@
     joined_k = jnp.concatenate(key_tiles, axis=1)
     joined_v = jnp.concatenate(value_tiles, axis=1)
     head_sum = jnp.concatenate(
-        [dot(joined_k, ski[pl.ds(0, half), :]), dot(joined_v, svi[pl.ds(0, half), :])], axis=1
+        [dot_t(joined_k, ski[:, pl.ds(0, half)]), dot_t(joined_v, svi[:, pl.ds(0, half)])], axis=1
     )
     tail_sum = jnp.concatenate(
-        [dot(joined_k, ski[pl.ds(half, half), :]), dot(joined_v, svi[pl.ds(half, half), :])], axis=1
+        [dot_t(joined_k, ski[:, pl.ds(half, half)]), dot_t(joined_v, svi[:, pl.ds(half, half)])], axis=1
     )
     row_c = lax.broadcasted_iota(jnp.int32, (cmp_rows, LANES), 0)
     shifted = jnp.where(row_c < cmp_rows - 1, pltpu.roll(tail_sum, cmp_rows - 1, 0), 0.0)
@@ -164,8 +237,6 @@
         return carry
 
     lax.fori_loop(me + 1, spans, clear, 0)
-
-    pl.semaphore_wait(barrier, spans)
 
     def pre_copy(source, target):
         return pltpu.make_async_remote_copy(
@@ -177,26 +248,11 @@
             device_id_type=MESH,
         )
 
-    def kv_copy(source, target):
-        return pltpu.make_async_remote_copy(
-            src_ref=kv_all.at[source],
-            dst_ref=kv_all.at[source],
-            send_sem=kv_send.at[target],
-            recv_sem=kv_recv.at[source],
-            device_id={"kv": target},
-            device_id_type=MESH,
-        )
-
     def send_pre(step, carry):
         pre_copy(me, spans - 1 - step).start()
         return carry
 
-    def send_kv(step, carry):
-        kv_copy(me, spans - 1 - step).start()
-        return carry
-
     lax.fori_loop(0, spans - 1 - me, send_pre, 0)
-    lax.fori_loop(0, spans - 1 - me, send_kv, 0)
 
     for load in loads[7:9]:
         load.wait()
@@ -207,17 +263,17 @@
         odd = jnp.where(low, swap(tile), 0.0).astype(BF16)
         q_s[:, pl.ds(2 * a * SEL, SEL), :] = even.reshape(blocks, SEL, LANES)
         q_s[:, pl.ds((2 * a + 1) * SEL, SEL), :] = odd.reshape(blocks, SEL, LANES)
-    gate_all = jax.nn.sigmoid(dot(tokens[...], wg[...]))
+    gate_all = jax.nn.sigmoid(dot_t(tokens[...], wg[...]))
     width = 2 * heads
     gates[...] = jnp.where(first, gate_all[:, :width], gate_all[:, width : 2 * width])
 
-    def set_bias(span):
-        ids = span * blocks + lax.broadcasted_iota(jnp.int32, (blocks, rows), 1) // SEL
-        picks = chosen_ref[:, 0, :]
-        hit = jnp.zeros((blocks, rows), F32)
+    picks = chosen_ref[:, 0, :]
+
+    def bias_of(ids):
+        hit = jnp.zeros((blocks, ids.shape[1]), F32)
         for t in range(picks.shape[1]):
             hit = jnp.where(picks[:, t : t + 1] == ids, 1.0, hit)
-        bias[...] = jnp.where(hit > 0.0, 0.0, NEG)
+        return jnp.where(hit > 0.0, 0.0, NEG)
 
     def lane_sum(p):
         total = p[:, :LANES]
@@ -225,41 +281,59 @@
             total = total + p[:, c * LANES : (c + 1) * LANES]
         return total
 
-    set_bias(me)
-
-    def own_block(j, carry):
-        keys = kv_all[me]
+    bias[...] = bias_of(me * blocks + lax.broadcasted_iota(jnp.int32, (blocks, rows), 1) // SEL)
+    slots[...] = block_of_slot(picks)
+    low_b = low_lanes((blocks, LANES))
+
+    def set_bias(span, carry):
+        ids = slots[pl.ds(span * CAP, CAP), :]
+        tiles = [
+            jnp.where(low_b, ids[2 * a : 2 * a + 1], ids[2 * a + 1 : 2 * a + 2])
+            for a in range(CAP // 2)
+        ]
+        far_bias[span] = bias_of(jnp.concatenate(tiles, axis=1))
+        return carry
+
+    lax.fori_loop(0, me, set_bias, 0)
+
+    def own_values(j):
+        keys = kv_own[...]
         scores = dot_t(q_s[j], keys) + bias[pl.ds(j, 1), :]
         place = lax.broadcasted_iota(jnp.int32, scores.shape, 1)
         time = j * SEL + lax.broadcasted_iota(jnp.int32, scores.shape, 0) % SEL
         scores = jnp.where(place <= time, scores, NEG)
         peak = jnp.max(scores, axis=1, keepdims=True)
         p = jnp.exp(scores - peak)
-        m_s[j] = jnp.broadcast_to(peak, (q_rows, LANES))
-        l_s[j] = lane_sum(p)
-        acc[j] = dot(p.astype(BF16), keys)
-        return carry
-
-    lax.fori_loop(0, blocks, own_block, 0)
+        return jnp.broadcast_to(peak, (q_rows, LANES)), lane_sum(p), dot(p.astype(BF16), keys)
+
+    def in_pairs(values):
+        def step(jj, carry):
+            both = (2 * jj, 2 * jj + 1)
+            for j, (peak, weight, total) in zip(both, [values(j) for j in both]):
+                m_s[j] = peak
+                l_s[j] = weight
+                acc[j] = total
+            return carry
+
+        lax.fori_loop(0, blocks // 2, step, 0)
+
+    in_pairs(own_values)
 
     def span_step(step, carry):
         span = me - 1 - step
-        set_bias(span)
         kv_copy(span, me).wait_recv()
 
-        def block(j, inner):
+        def far_values(j):
             keys = kv_all[span]
-            scores = dot_t(q_s[j], keys) + bias[pl.ds(j, 1), :]
+            scores = dot_t(q_s[j], keys) + far_bias[span, pl.ds(j, 1), :]
             old = m_s[j]
             peak = jnp.maximum(old, jnp.max(scores, axis=1, keepdims=True))
             p = jnp.exp(scores - peak[:, :1])
             fix = jnp.exp(old - peak)
-            m_s[j] = peak
-            l_s[j] = l_s[j] * fix + lane_sum(p)
-            acc[j] = acc[j] * fix + dot(p.astype(BF16), keys)
-            return inner
-
-        return lax.fori_loop(0, blocks, block, carry)
+            return peak, l_s[j] * fix + lane_sum(p), acc[j] * fix + dot(p.astype(BF16), keys)
+
+        in_pairs(far_values)
+        return carry
 
     lax.fori_loop(0, me, span_step, 0)
 
@@ -296,7 +370,7 @@
             device_id_type=MESH,
         )
 
-    def finish_block(j, carry):
+    def finished(j):
         table = sum_kv[...]
         scores = dot_t(q_s[j], table)
         ends = lax.broadcasted_iota(jnp.int32, scores.shape, 1) * CMP_STRIDE + CMP_LEN - 1
@@ -319,11 +393,17 @@
         tiles = [
             jnp.where(low_q, swap(heads_out[2 * a]), heads_out[2 * a + 1]) for a in range(heads // 2)
         ]
-        mixed_own[part, :] = jnp.concatenate(tiles, axis=1).astype(BF16)
-        mix_copy(j).start()
-        return carry
-
-    lax.fori_loop(0, blocks, finish_block, 0)
+        return part, jnp.concatenate(tiles, axis=1).astype(BF16)
+
+    def finish_pair(jj, carry):
+        both = (2 * jj, 2 * jj + 1)
+        for part, mixed in [finished(j) for j in both]:
+            mixed_own[part, :] = mixed
+        for j in both:
+            mix_copy(j).start()
+        return carry
+
+    lax.fori_loop(0, blocks // 2, finish_pair, 0)
     loads[11].wait()
 
     half_rows = heads * HEAD
@@ -359,6 +439,12 @@
         return carry
 
     lax.fori_loop(0, spans - 1 - me, end_sends, 0)
+
+    def end_asks(span, carry):
+        ask_copy(me, span).wait_send()
+        return carry
+
+    lax.fori_loop(0, me, end_asks, 0)
 
 
 def local(spans, tokens, chosen, *weights):
@@ -380,25 +466,32 @@
             pltpu.VMEM(w_query.shape, BF16),
             pltpu.VMEM((width, 2 * w_ks.shape[1]), BF16),
             pltpu.VMEM((width, 2 * w_kc.shape[1]), BF16),
-            pltpu.VMEM(ski.shape, BF16),
+            pltpu.VMEM(ski.shape[::-1], BF16),
             pltpu.VMEM(sko.shape, BF16),
-            pltpu.VMEM(svi.shape, BF16),
+            pltpu.VMEM(svi.shape[::-1], BF16),
             pltpu.VMEM(svo.shape, BF16),
-            pltpu.VMEM(w_gates.shape, BF16),
+            pltpu.VMEM(w_gates.shape[::-1], BF16),
             pltpu.VMEM(w_out.shape, BF16),
             pltpu.VMEM((rows, LANES), F32),
-            pltpu.VMEM((spans, rows, LANES), BF16),
+            pltpu.VMEM((rows, LANES), BF16),
+            pltpu.VMEM((spans, CAP * SEL, LANES), BF16),
+            pltpu.VMEM((spans, CAP * SEL, LANES), BF16),
+            pltpu.VMEM((spans,) + chosen.shape, jnp.int32),
+            pltpu.VMEM((spans * CAP, LANES), jnp.int32),
             pltpu.VMEM((spans, cmp_rows + 8, LANES), F32),
             pltpu.VMEM((spans * cmp_rows, LANES), BF16),
             pltpu.VMEM((blocks, heads * SEL, LANES), BF16),
             pltpu.VMEM((rows, 2 * heads), F32),
             pltpu.VMEM((blocks, rows), F32),
+            pltpu.VMEM((spans, blocks, CAP * SEL), F32),
             pltpu.VMEM((blocks, heads * SEL, LANES), F32),
             pltpu.VMEM((blocks, heads * SEL, LANES), F32),
             pltpu.VMEM((blocks, heads * SEL, LANES), F32),
             pltpu.VMEM((rows, heads * HEAD), BF16),
             pltpu.VMEM((rows, heads * HEAD), BF16),
             dma((12,)),
+            dma((spans,)),
+            dma((spans,)),
             dma((spans,)),
             dma((spans,)),
             dma((spans,)),
@@ -415,11 +508,11 @@
         w_vs,
         w_kc,
         w_vc,
-        ski,
+        ski.T,
         sko,
-        svi,
+        svi.T,
         svo,
-        w_gates,
+        w_gates.T,
         w_out,
         gain.reshape(1, -1),
     )

time: 39.9 us -> 29.7 us (0.74)
  Pallas kernels: 34.2 us -> 27.6 us
  local copies, waits for them, and re-layouts: 5.53 us -> 1.87 us
    pallas_call x1, Pallas kernels: 34.2 us -> 27.6 us  [local(): pl.pallas_call(functools.partial(kernel, spans), out_shape=jax.ShapeDtype...]
    unnamed x8 -> x1, local copies, waits for them, and re-layouts: 5.53 us -> 1.87 us
where the time goes in v2:
time: 29.7 us; the launch traced here: 29.5 us
  Pallas kernels  27.6 us (93%)
  local copies, waits for them, and re-layouts  1.87 us (6%)
    pallas_call x1, Pallas kernels, local(): pl.pallas_call(functools.partial(kernel, spans), out_shape=jax.ShapeDtype...  27.6 us
    unnamed x1, local copies, waits for them, and re-layouts  1.87 us

profile of v2, /device:TPU:19, one launch (start us, length us, event | category | flops | bytes accessed | tf_op | source)
XLA Modules:
  0.0 29.5 jit_solution(9696253275505300146)
XLA Ops:
  0.0 27.6 %shard_map.136 = bf16[512,512]{1,0:T(8,128)(2,1)} custom-call(bf16[512,1024]{1,0:T(8,128)(2,1)} %tokens_h.1, s32[8,1,16]{2,1,0:T(1,128)} %chosen_ref.1, bf16[1024,256]{1,0:T(8,128)(2,1)} %wq_h.1, bf16[1024,128]{1,0:T(8,128)(2,1)} %wks_h.1, bf16[1024,128]{1,0:T(8,128)(2,1)} %wvs_h.1, bf16[1024,128]{1,0:T(8,128)(2,1)} %wkc_h.1, bf16[1024,128]{1,0:T(8,128)(2,1)} %wvc_h.1, ...), custom_call_target="tpu_custom_call" | custom-call | tf_op jit(solution)/shard_map/pallas_call | solution.py:459
  27.6 1.9 %copy.16 = bf16[512,512]{1,0:T(8,128)(2,1)} copy(bf16[512,512]{1,0:T(8,128)(2,1)} %shard_map.136) | data formatting | bytes 1048576

commit v3 on v2

--- a/solution.py
+++ b/solution.py
@@ -12,6 +12,7 @@
 CMP_LEN = 32
 SEL = 64
 CAP = 4
+FAR = 3
 LANES = 128
 EPS = 1e-06
 NEG = -1e30
@@ -78,6 +79,8 @@
     acc,
     m_s,
     l_s,
+    sum_out,
+    gate_s,
     mixed_own,
     mixed_other,
     in_sem,
@@ -98,6 +101,8 @@
     cmp_rows = rows // CMP_STRIDE
     heads = wq.shape[1] // HEAD
     q_rows = heads * SEL
+    chunks, far_keys = far_bias.shape[0], far_bias.shape[2]
+    per_chunk = far_keys // (CAP * SEL)
 
     loads = [
         pltpu.make_async_copy(src, dst, in_sem.at[i])
@@ -173,10 +178,10 @@
         for d in range(1, blocks):
             rank = rank + jnp.where(lane % blocks >= d, pltpu.roll(need, d, 1), 0)
         code = jnp.where((need > 0) & (rank < CAP), lane // blocks * CAP + rank, -1)[:1]
-        place = lax.broadcasted_iota(jnp.int32, (spans * CAP, lanes), 0)
-        id_row = lax.broadcasted_iota(jnp.int32, (spans * CAP, lanes), 1)
+        place = lax.broadcasted_iota(jnp.int32, (slots.shape[0], lanes), 0)
+        id_row = lax.broadcasted_iota(jnp.int32, (slots.shape[0], lanes), 1)
         found = jnp.where(code == place, id_row, -1)
-        return jnp.broadcast_to(jnp.max(found, axis=1, keepdims=True), (spans * CAP, LANES))
+        return jnp.broadcast_to(jnp.max(found, axis=1, keepdims=True), slots.shape)
 
     def pair(both):
         k2, v2 = both[:, :LANES], both[:, LANES:]
@@ -187,23 +192,6 @@
     for load in loads[:3]:
         load.wait()
     kv_own[...] = pair(dot(tokens[...], wcho[...])).astype(BF16)
-
-    def serve(step, carry):
-        target = spans - 1 - step
-        ask_copy(target, me).wait_recv()
-        slots[...] = block_of_slot(asks[target][:, 0, :])
-        key_lane = lax.broadcasted_iota(jnp.int32, (SEL, rows), 1)
-        key_row = lax.broadcasted_iota(jnp.int32, (SEL, rows), 0)
-        ours = slots[pl.ds(me * CAP, CAP), :]
-        pieces = []
-        for k in range(CAP):
-            start = (ours[k : k + 1, :1] - me * blocks) * SEL
-            pieces.append(jnp.where(key_lane == start + key_row, 1.0, 0.0).astype(BF16))
-        packed[target] = dot(jnp.concatenate(pieces, axis=0), kv_own[...]).astype(BF16)
-        kv_copy(me, target).start()
-        return carry
-
-    lax.fori_loop(0, spans - 1 - me, serve, 0)
 
     for load in loads[3:5]:
         load.wait()
@@ -254,6 +242,23 @@
 
     lax.fori_loop(0, spans - 1 - me, send_pre, 0)
 
+    def serve(step, carry):
+        target = spans - 1 - step
+        ask_copy(target, me).wait_recv()
+        slots[...] = block_of_slot(asks[target][:, 0, :])
+        key_lane = lax.broadcasted_iota(jnp.int32, (SEL, rows), 1)
+        key_row = lax.broadcasted_iota(jnp.int32, (SEL, rows), 0)
+        ours = slots[pl.ds(me * CAP, CAP), :]
+        pieces = []
+        for k in range(CAP):
+            start = (ours[k : k + 1, :1] - me * blocks) * SEL
+            pieces.append(jnp.where(key_lane == start + key_row, 1.0, 0.0).astype(BF16))
+        packed[target] = dot(jnp.concatenate(pieces, axis=0), kv_own[...]).astype(BF16)
+        kv_copy(me, target).start()
+        return carry
+
+    lax.fori_loop(0, spans - 1 - me, serve, 0)
+
     for load in loads[7:9]:
         load.wait()
     scaled = dot(tokens[...], wq[...]).astype(BF16).astype(F32) * (HEAD**-0.5)
@@ -284,58 +289,36 @@
     bias[...] = bias_of(me * blocks + lax.broadcasted_iota(jnp.int32, (blocks, rows), 1) // SEL)
     slots[...] = block_of_slot(picks)
     low_b = low_lanes((blocks, LANES))
-
-    def set_bias(span, carry):
-        ids = slots[pl.ds(span * CAP, CAP), :]
-        tiles = [
-            jnp.where(low_b, ids[2 * a : 2 * a + 1], ids[2 * a + 1 : 2 * a + 2])
-            for a in range(CAP // 2)
-        ]
-        far_bias[span] = bias_of(jnp.concatenate(tiles, axis=1))
-        return carry
-
-    lax.fori_loop(0, me, set_bias, 0)
-
-    def own_values(j):
-        keys = kv_own[...]
-        scores = dot_t(q_s[j], keys) + bias[pl.ds(j, 1), :]
-        place = lax.broadcasted_iota(jnp.int32, scores.shape, 1)
-        time = j * SEL + lax.broadcasted_iota(jnp.int32, scores.shape, 0) % SEL
-        scores = jnp.where(place <= time, scores, NEG)
-        peak = jnp.max(scores, axis=1, keepdims=True)
-        p = jnp.exp(scores - peak)
-        return jnp.broadcast_to(peak, (q_rows, LANES)), lane_sum(p), dot(p.astype(BF16), keys)
-
-    def in_pairs(values):
-        def step(jj, carry):
-            both = (2 * jj, 2 * jj + 1)
-            for j, (peak, weight, total) in zip(both, [values(j) for j in both]):
-                m_s[j] = peak
-                l_s[j] = weight
-                acc[j] = total
-            return carry
-
-        lax.fori_loop(0, blocks // 2, step, 0)
-
-    in_pairs(own_values)
-
-    def span_step(step, carry):
-        span = me - 1 - step
-        kv_copy(span, me).wait_recv()
-
-        def far_values(j):
-            keys = kv_all[span]
-            scores = dot_t(q_s[j], keys) + far_bias[span, pl.ds(j, 1), :]
-            old = m_s[j]
-            peak = jnp.maximum(old, jnp.max(scores, axis=1, keepdims=True))
-            p = jnp.exp(scores - peak[:, :1])
-            fix = jnp.exp(old - peak)
-            return peak, l_s[j] * fix + lane_sum(p), acc[j] * fix + dot(p.astype(BF16), keys)
-
-        in_pairs(far_values)
-        return carry
-
-    lax.fori_loop(0, me, span_step, 0)
+    for c in range(chunks):
+        tiles = []
+        for span in range(c * per_chunk, (c + 1) * per_chunk):
+            ids = slots[pl.ds(span * CAP, CAP), :]
+            ids = jnp.where(span < me, ids, -1)
+            for a in range(CAP // 2):
+                tiles.append(jnp.where(low_b, ids[2 * a : 2 * a + 1], ids[2 * a + 1 : 2 * a + 2]))
+        far_bias[c] = bias_of(jnp.concatenate(tiles, axis=1))
+
+    def clear_far(span, carry):
+        kv_all[span] = jnp.zeros(kv_all.shape[1:], BF16)
+        return carry
+
+    lax.fori_loop(me, chunks * per_chunk, clear_far, 0)
+
+    lane_q = lax.broadcasted_iota(jnp.int32, (q_rows, LANES), 1)
+    row_q = lax.broadcasted_iota(jnp.int32, (q_rows, LANES), 0) % SEL
+    for jj in range(blocks // 2):
+        keys = kv_own[: (jj + 1) * 2 * SEL]
+        for odd in range(2):
+            j = 2 * jj + odd
+            scores = dot_t(q_s[j], keys) + bias[j : j + 1, : keys.shape[0]]
+            tail = jnp.where(lane_q <= row_q + odd * SEL, scores[:, -LANES:], NEG)
+            if jj > 0:
+                tail = jnp.concatenate([scores[:, :-LANES], tail], axis=1)
+            peak = jnp.max(tail, axis=1, keepdims=True)
+            p = jnp.exp(tail - peak)
+            m_s[j] = jnp.broadcast_to(peak, (q_rows, LANES))
+            l_s[j] = lane_sum(p)
+            acc[j] = dot(p.astype(BF16), keys)
 
     def await_pre(span, carry):
         pre_copy(span, me).wait_recv()
@@ -357,6 +340,65 @@
         [dot(hidden[:, :HEAD], sko[...]), dot(hidden[:, HEAD:], svo[...])], axis=1
     ).astype(BF16)
 
+    def summarized(j):
+        table = sum_kv[...]
+        scores = dot_t(q_s[j], table)
+        ends = lax.broadcasted_iota(jnp.int32, scores.shape, 1) * CMP_STRIDE + CMP_LEN - 1
+        time = me * rows + j * SEL + lax.broadcasted_iota(jnp.int32, scores.shape, 0) % SEL
+        visible = ends <= time
+        scores = jnp.where(visible, scores, NEG)
+        peak = jnp.max(scores, axis=1, keepdims=True)
+        p = jnp.where(visible, jnp.exp(scores - peak), 0.0)
+        weight = jnp.sum(p, axis=1, keepdims=True)
+        gate = gates[pl.ds(pl.multiple_of(j * SEL, SEL), SEL), :]
+        near = jnp.concatenate([gate[:, 2 * h : 2 * h + 1] for h in range(heads)], axis=0)
+        far = jnp.concatenate([gate[:, 2 * h + 1 : 2 * h + 2] for h in range(heads)], axis=0)
+        factor = near / jnp.where(weight > 0.0, weight, 1.0)
+        return dot(p.astype(BF16), table) * factor, jnp.broadcast_to(far, (q_rows, LANES))
+
+    def summary_pair(jj, carry):
+        both = (2 * jj, 2 * jj + 1)
+        for j, (total, far) in zip(both, [summarized(j) for j in both]):
+            sum_out[j] = total
+            gate_s[j] = far
+        return carry
+
+    lax.fori_loop(0, blocks // 2, summary_pair, 0)
+
+    def merged(j, chunk):
+        keys = kv_all[pl.ds(chunk * per_chunk, per_chunk)].reshape(far_keys, LANES)
+        scores = dot_t(q_s[j], keys) + far_bias[chunk, pl.ds(j, 1), :]
+        old = m_s[j]
+        peak = jnp.maximum(old, jnp.max(scores, axis=1, keepdims=True))
+        p = jnp.concatenate(
+            [jnp.exp(scores[:, c : c + LANES] - peak) for c in range(0, far_keys, LANES)], axis=1
+        )
+        fix = jnp.exp(old - peak)
+        return peak, l_s[j] * fix + lane_sum(p), acc[j] * fix + dot(p.astype(BF16), keys)
+
+    def await_far(span, carry):
+        kv_copy(span, me).wait_recv()
+        return carry
+
+    def chunk_step(step, carry):
+        chunk = chunks - 1 - step
+        lax.fori_loop(
+            chunk * per_chunk, jnp.minimum((chunk + 1) * per_chunk, me), await_far, 0
+        )
+
+        def update(j, inner):
+            peak, weight, total = merged(j, chunk)
+            m_s[j] = peak
+            l_s[j] = weight
+            acc[j] = total
+            return inner
+
+        return lax.fori_loop(0, blocks, update, carry)
+
+    if chunks > 1:
+        lax.fori_loop(0, chunks - 1, chunk_step, 0)
+
+    lax.fori_loop(0, jnp.minimum(per_chunk, me), await_far, 0)
     low_q = low_lanes((SEL, LANES))
 
     def mix_copy(j):
@@ -371,28 +413,14 @@
         )
 
     def finished(j):
-        table = sum_kv[...]
-        scores = dot_t(q_s[j], table)
-        ends = lax.broadcasted_iota(jnp.int32, scores.shape, 1) * CMP_STRIDE + CMP_LEN - 1
-        time = me * rows + j * SEL + lax.broadcasted_iota(jnp.int32, scores.shape, 0) % SEL
-        visible = ends <= time
-        scores = jnp.where(visible, scores, NEG)
-        peak = jnp.max(scores, axis=1, keepdims=True)
-        p = jnp.where(visible, jnp.exp(scores - peak), 0.0)
-        weight = jnp.sum(p, axis=1, keepdims=True)
-        summary = dot(p.astype(BF16), table) / jnp.where(weight > 0.0, weight, 1.0)
-        picked = acc[j] / jnp.sum(l_s[j], axis=1, keepdims=True)
+        _, weight, total = merged(j, 0)
+        mixed = sum_out[j] + total * (gate_s[j] / jnp.sum(weight, axis=1, keepdims=True))
         part = pl.ds(pl.multiple_of(j * SEL, SEL), SEL)
-        gate = gates[part, :]
-        heads_out = []
-        for h in range(heads):
-            cut = slice(h * SEL, (h + 1) * SEL)
-            heads_out.append(
-                gate[:, 2 * h : 2 * h + 1] * summary[cut] + gate[:, 2 * h + 1 : 2 * h + 2] * picked[cut]
-            )
-        tiles = [
-            jnp.where(low_q, swap(heads_out[2 * a]), heads_out[2 * a + 1]) for a in range(heads // 2)
-        ]
+        tiles = []
+        for a in range(heads // 2):
+            even = mixed[2 * a * SEL : (2 * a + 1) * SEL]
+            odd = mixed[(2 * a + 1) * SEL : (2 * a + 2) * SEL]
+            tiles.append(jnp.where(low_q, swap(even), odd))
         return part, jnp.concatenate(tiles, axis=1).astype(BF16)
 
     def finish_pair(jj, carry):
@@ -453,6 +481,8 @@
     heads = w_query.shape[1] // HEAD
     blocks = rows // SEL
     cmp_rows = rows // CMP_STRIDE
+    per_chunk = min(FAR, spans - 1)
+    chunks = -(-(spans - 1) // per_chunk)
     any_spec = pl.BlockSpec(memory_space=pl.ANY)
     vmem = pl.BlockSpec(memory_space=pltpu.VMEM)
     dma = pltpu.SemaphoreType.DMA
@@ -474,16 +504,18 @@
             pltpu.VMEM(w_out.shape, BF16),
             pltpu.VMEM((rows, LANES), F32),
             pltpu.VMEM((rows, LANES), BF16),
-            pltpu.VMEM((spans, CAP * SEL, LANES), BF16),
+            pltpu.VMEM((chunks * per_chunk, CAP * SEL, LANES), BF16),
             pltpu.VMEM((spans, CAP * SEL, LANES), BF16),
             pltpu.VMEM((spans,) + chosen.shape, jnp.int32),
-            pltpu.VMEM((spans * CAP, LANES), jnp.int32),
+            pltpu.VMEM((max(spans, chunks * per_chunk) * CAP, LANES), jnp.int32),
             pltpu.VMEM((spans, cmp_rows + 8, LANES), F32),
             pltpu.VMEM((spans * cmp_rows, LANES), BF16),
             pltpu.VMEM((blocks, heads * SEL, LANES), BF16),
             pltpu.VMEM((rows, 2 * heads), F32),
             pltpu.VMEM((blocks, rows), F32),
-            pltpu.VMEM((spans, blocks, CAP * SEL), F32),
+            pltpu.VMEM((chunks, blocks, per_chunk * CAP * SEL), F32),
+            pltpu.VMEM((blocks, heads * SEL, LANES), F32),
+            pltpu.VMEM((blocks, heads * SEL, LANES), F32),
             pltpu.VMEM((blocks, heads * SEL, LANES), F32),
             pltpu.VMEM((blocks, heads * SEL, LANES), F32),
             pltpu.VMEM((blocks, heads * SEL, LANES), F32),

time: 29.7 us -> 25.3 us (0.85)
  the two profiles are of different devices: /device:TPU:19 before, /device:TPU:0 now
where the time goes in v3:
time: 25.3 us; the launch traced here: 25.1 us
  Pallas kernels  23.2 us (92%)
  local copies, waits for them, and re-layouts  1.87 us (7%)
    pallas_call x1, Pallas kernels, local(): pl.pallas_call(functools.partial(kernel, spans), out_shape=jax.ShapeDtype...  23.2 us
    unnamed x1, local copies, waits for them, and re-layouts  1.87 us

profile of v3, /device:TPU:0, one launch (start us, length us, event | category | flops | bytes accessed | tf_op | source)
XLA Modules:
  0.0 25.1 jit_solution(6965075994731718192)
XLA Ops:
  0.0 23.2 %shard_map.136 = bf16[512,512]{1,0:T(8,128)(2,1)} custom-call(bf16[512,1024]{1,0:T(8,128)(2,1)} %tokens_h.1, s32[8,1,16]{2,1,0:T(1,128)} %chosen_ref.1, bf16[1024,256]{1,0:T(8,128)(2,1)} %wq_h.1, bf16[1024,128]{1,0:T(8,128)(2,1)} %wks_h.1, bf16[1024,128]{1,0:T(8,128)(2,1)} %wvs_h.1, bf16[1024,128]{1,0:T(8,128)(2,1)} %wkc_h.1, bf16[1024,128]{1,0:T(8,128)(2,1)} %wvc_h.1, ...), custom_call_target="tpu_custom_call" | custom-call | tf_op jit(solution)/shard_map/pallas_call | solution.py:489
  23.2 1.9 %copy.16 = bf16[512,512]{1,0:T(8,128)(2,1)} copy(bf16[512,512]{1,0:T(8,128)(2,1)} %shard_map.136) | data formatting | bytes 1048576

commit v4 on v3

--- a/solution.py
+++ b/solution.py
@@ -13,6 +13,7 @@
 SEL = 64
 CAP = 4
 FAR = 3
+WIDE = 4
 LANES = 128
 EPS = 1e-06
 NEG = -1e30
@@ -158,13 +159,15 @@
             device_id_type=MESH,
         )
 
-    pl.semaphore_wait(barrier, spans)
-
     def send_ask(span, carry):
         ask_copy(me, span).start()
         return carry
 
-    lax.fori_loop(0, me, send_ask, 0)
+    def enter():
+        pl.semaphore_wait(barrier, spans)
+        lax.fori_loop(0, me, send_ask, 0)
+
+    pl.when(me >= spans // 2)(enter)
 
     def block_of_slot(picks):
         lanes = -(-spans * blocks // LANES) * LANES
@@ -236,11 +239,61 @@
             device_id_type=MESH,
         )
 
+    pl.when(me < spans // 2)(enter)
+
     def send_pre(step, carry):
         pre_copy(me, spans - 1 - step).start()
         return carry
 
     lax.fori_loop(0, spans - 1 - me, send_pre, 0)
+
+
+    for load in loads[7:9]:
+        load.wait()
+    scaled = dot(tokens[...], wq[...]).astype(BF16).astype(F32) * (HEAD**-0.5)
+    for a in range(heads // 2):
+        tile = scaled[:, a * LANES : (a + 1) * LANES]
+        even = jnp.where(low, tile, 0.0).astype(BF16)
+        odd = jnp.where(low, swap(tile), 0.0).astype(BF16)
+        q_s[:, pl.ds(2 * a * SEL, SEL), :] = even.reshape(blocks, SEL, LANES)
+        q_s[:, pl.ds((2 * a + 1) * SEL, SEL), :] = odd.reshape(blocks, SEL, LANES)
+    gate_all = jax.nn.sigmoid(dot_t(tokens[...], wg[...]))
+    width = 2 * heads
+    gates[...] = jnp.where(first, gate_all[:, :width], gate_all[:, width : 2 * width])
+
+    picks = chosen_ref[:, 0, :]
+
+    def bias_of(ids):
+        hit = jnp.zeros((blocks, ids.shape[1]), F32)
+        for t in range(picks.shape[1]):
+            hit = jnp.where(picks[:, t : t + 1] == ids, 1.0, hit)
+        return jnp.where(hit > 0.0, 0.0, NEG)
+
+    def lane_sum(p):
+        total = p[:, :LANES]
+        for c in range(1, p.shape[1] // LANES):
+            total = total + p[:, c * LANES : (c + 1) * LANES]
+        return total
+
+    def own_attention():
+        bias[...] = bias_of(me * blocks + lax.broadcasted_iota(jnp.int32, (blocks, rows), 1) // SEL)
+        lane_q = lax.broadcasted_iota(jnp.int32, (q_rows, LANES), 1)
+        row_q = lax.broadcasted_iota(jnp.int32, (q_rows, LANES), 0) % SEL
+        for jj in range(blocks // 2):
+            keys = kv_own[: (jj + 1) * 2 * SEL]
+            for odd in range(2):
+                j = 2 * jj + odd
+                scores = dot_t(q_s[j], keys) + bias[j : j + 1, : keys.shape[0]]
+                tail = jnp.where(lane_q <= row_q + odd * SEL, scores[:, -LANES:], NEG)
+                if jj > 0:
+                    tail = jnp.concatenate([scores[:, :-LANES], tail], axis=1)
+                peak = jnp.max(tail, axis=1, keepdims=True)
+                p = jnp.exp(tail - peak)
+                m_s[j] = jnp.broadcast_to(peak, (q_rows, LANES))
+                l_s[j] = lane_sum(p)
+                acc[j] = dot(p.astype(BF16), keys)
+
+    pl.when(me == 0)(own_attention)
 
     def serve(step, carry):
         target = spans - 1 - step
@@ -259,34 +312,8 @@
 
     lax.fori_loop(0, spans - 1 - me, serve, 0)
 
-    for load in loads[7:9]:
-        load.wait()
-    scaled = dot(tokens[...], wq[...]).astype(BF16).astype(F32) * (HEAD**-0.5)
-    for a in range(heads // 2):
-        tile = scaled[:, a * LANES : (a + 1) * LANES]
-        even = jnp.where(low, tile, 0.0).astype(BF16)
-        odd = jnp.where(low, swap(tile), 0.0).astype(BF16)
-        q_s[:, pl.ds(2 * a * SEL, SEL), :] = even.reshape(blocks, SEL, LANES)
-        q_s[:, pl.ds((2 * a + 1) * SEL, SEL), :] = odd.reshape(blocks, SEL, LANES)
-    gate_all = jax.nn.sigmoid(dot_t(tokens[...], wg[...]))
-    width = 2 * heads
-    gates[...] = jnp.where(first, gate_all[:, :width], gate_all[:, width : 2 * width])
-
-    picks = chosen_ref[:, 0, :]
-
-    def bias_of(ids):
-        hit = jnp.zeros((blocks, ids.shape[1]), F32)
-        for t in range(picks.shape[1]):
-            hit = jnp.where(picks[:, t : t + 1] == ids, 1.0, hit)
-        return jnp.where(hit > 0.0, 0.0, NEG)
-
-    def lane_sum(p):
-        total = p[:, :LANES]
-        for c in range(1, p.shape[1] // LANES):
-            total = total + p[:, c * LANES : (c + 1) * LANES]
-        return total
-
-    bias[...] = bias_of(me * blocks + lax.broadcasted_iota(jnp.int32, (blocks, rows), 1) // SEL)
+    pl.when(me > 0)(own_attention)
+
     slots[...] = block_of_slot(picks)
     low_b = low_lanes((blocks, LANES))
     for c in range(chunks):
@@ -303,22 +330,6 @@
         return carry
 
     lax.fori_loop(me, chunks * per_chunk, clear_far, 0)
-
-    lane_q = lax.broadcasted_iota(jnp.int32, (q_rows, LANES), 1)
-    row_q = lax.broadcasted_iota(jnp.int32, (q_rows, LANES), 0) % SEL
-    for jj in range(blocks // 2):
-        keys = kv_own[: (jj + 1) * 2 * SEL]
-        for odd in range(2):
-            j = 2 * jj + odd
-            scores = dot_t(q_s[j], keys) + bias[j : j + 1, : keys.shape[0]]
-            tail = jnp.where(lane_q <= row_q + odd * SEL, scores[:, -LANES:], NEG)
-            if jj > 0:
-                tail = jnp.concatenate([scores[:, :-LANES], tail], axis=1)
-            peak = jnp.max(tail, axis=1, keepdims=True)
-            p = jnp.exp(tail - peak)
-            m_s[j] = jnp.broadcast_to(peak, (q_rows, LANES))
-            l_s[j] = lane_sum(p)
-            acc[j] = dot(p.astype(BF16), keys)
 
     def await_pre(span, carry):
         pre_copy(span, me).wait_recv()
@@ -350,20 +361,17 @@
         peak = jnp.max(scores, axis=1, keepdims=True)
         p = jnp.where(visible, jnp.exp(scores - peak), 0.0)
         weight = jnp.sum(p, axis=1, keepdims=True)
-        gate = gates[pl.ds(pl.multiple_of(j * SEL, SEL), SEL), :]
+        gate = gates[j * SEL : (j + 1) * SEL, :]
         near = jnp.concatenate([gate[:, 2 * h : 2 * h + 1] for h in range(heads)], axis=0)
         far = jnp.concatenate([gate[:, 2 * h + 1 : 2 * h + 2] for h in range(heads)], axis=0)
         factor = near / jnp.where(weight > 0.0, weight, 1.0)
         return dot(p.astype(BF16), table) * factor, jnp.broadcast_to(far, (q_rows, LANES))
 
-    def summary_pair(jj, carry):
-        both = (2 * jj, 2 * jj + 1)
-        for j, (total, far) in zip(both, [summarized(j) for j in both]):
+    for start in range(0, blocks, WIDE):
+        some = range(start, start + WIDE)
+        for j, (total, far) in zip(some, [summarized(j) for j in some]):
             sum_out[j] = total
             gate_s[j] = far
-        return carry
-
-    lax.fori_loop(0, blocks // 2, summary_pair, 0)
 
     def merged(j, chunk):
         keys = kv_all[pl.ds(chunk * per_chunk, per_chunk)].reshape(far_keys, LANES)
@@ -412,26 +420,26 @@
             device_id_type=MESH,
         )
 
-    def finished(j):
-        _, weight, total = merged(j, 0)
+    def finished(j, far):
+        _, weight, total = merged(j, 0) if far else (None, l_s[j], acc[j])
         mixed = sum_out[j] + total * (gate_s[j] / jnp.sum(weight, axis=1, keepdims=True))
-        part = pl.ds(pl.multiple_of(j * SEL, SEL), SEL)
         tiles = []
         for a in range(heads // 2):
             even = mixed[2 * a * SEL : (2 * a + 1) * SEL]
             odd = mixed[(2 * a + 1) * SEL : (2 * a + 2) * SEL]
             tiles.append(jnp.where(low_q, swap(even), odd))
-        return part, jnp.concatenate(tiles, axis=1).astype(BF16)
-
-    def finish_pair(jj, carry):
-        both = (2 * jj, 2 * jj + 1)
-        for part, mixed in [finished(j) for j in both]:
-            mixed_own[part, :] = mixed
-        for j in both:
-            mix_copy(j).start()
-        return carry
-
-    lax.fori_loop(0, blocks // 2, finish_pair, 0)
+        return jnp.concatenate(tiles, axis=1).astype(BF16)
+
+    def finish_all(far):
+        for start in range(0, blocks, WIDE):
+            some = range(start, start + WIDE)
+            for j, mixed in zip(some, [finished(j, far) for j in some]):
+                mixed_own[j * SEL : (j + 1) * SEL, :] = mixed
+            for j in some:
+                mix_copy(j).start()
+
+    pl.when(me == 0)(functools.partial(finish_all, False))
+    pl.when(me > 0)(functools.partial(finish_all, True))
     loads[11].wait()
 
     half_rows = heads * HEAD
@@ -441,19 +449,16 @@
     own_cols = pl.ds(pl.multiple_of(group * half_cols, half_cols), half_cols)
     other_cols = pl.ds(pl.multiple_of((1 - group) * half_cols, half_cols), half_cols)
 
-    def project_block(j, carry):
-        for b in range(2):
-            mix_copy(2 * j + b).wait_recv()
-        part = pl.ds(pl.multiple_of(2 * j * SEL, 2 * SEL), 2 * SEL)
+    gain = gain_ref[:, own_cols]
+    for start in range(0, blocks, WIDE):
+        for j in range(start, start + WIDE):
+            mix_copy(j).wait_recv()
+        part = pl.ds(start * SEL, WIDE * SEL)
         own, other = mixed_own[part, :], mixed_other[part, :]
         mine = dot(own, wo[own_rows, own_cols]) + dot(other, wo[other_rows, own_cols])
         rest = dot(own, wo[own_rows, other_cols]) + dot(other, wo[other_rows, other_cols])
         power = jnp.sum(mine * mine + rest * rest, axis=1, keepdims=True)
-        scale = lax.rsqrt(power / wo.shape[1] + EPS)
-        out_ref[part, :] = (mine * scale * gain_ref[:, own_cols]).astype(BF16)
-        return carry
-
-    lax.fori_loop(0, blocks // 2, project_block, 0)
+        out_ref[part, :] = (mine * lax.rsqrt(power / wo.shape[1] + EPS) * gain).astype(BF16)
 
     def end_mix(j, carry):
         mix_copy(j).wait_send()

time: 25.3 us -> 22.4 us (0.89)
  the two profiles are of different devices: /device:TPU:0 before, /device:TPU:11 now
where the time goes in v4:
time: 22.4 us; the launch traced here: 22.2 us
  Pallas kernels  20.3 us (91%)
  local copies, waits for them, and re-layouts  1.87 us (8%)
    pallas_call x1, Pallas kernels, local(): pl.pallas_call(functools.partial(kernel, spans), out_shape=jax.ShapeDtype...  20.3 us
    unnamed x1, local copies, waits for them, and re-layouts  1.87 us

profile of v4, /device:TPU:11, one launch (start us, length us, event | category | flops | bytes accessed | tf_op | source)
XLA Modules:
  0.0 22.2 jit_solution(5689110887918923251)
XLA Ops:
  0.0 20.3 %shard_map.136 = bf16[512,512]{1,0:T(8,128)(2,1)} custom-call(bf16[512,1024]{1,0:T(8,128)(2,1)} %tokens_h.1, s32[8,1,16]{2,1,0:T(1,128)} %chosen_ref.1, bf16[1024,256]{1,0:T(8,128)(2,1)} %wq_h.1, bf16[1024,128]{1,0:T(8,128)(2,1)} %wks_h.1, bf16[1024,128]{1,0:T(8,128)(2,1)} %wvs_h.1, bf16[1024,128]{1,0:T(8,128)(2,1)} %wkc_h.1, bf16[1024,128]{1,0:T(8,128)(2,1)} %wvc_h.1, ...), custom_call_target="tpu_custom_call" | custom-call | tf_op jit(solution)/shard_map/pallas_call | solution.py:494
  20.3 1.9 %copy.16 = bf16[512,512]{1,0:T(8,128)(2,1)} copy(bf16[512,512]{1,0:T(8,128)(2,1)} %shard_map.136) | data formatting | bytes 1048576

commit v5 on v4

--- a/solution.py
+++ b/solution.py
@@ -296,7 +296,7 @@
     pl.when(me == 0)(own_attention)
 
     def serve(step, carry):
-        target = spans - 1 - step
+        target = me + 1 + step
         ask_copy(target, me).wait_recv()
         slots[...] = block_of_slot(asks[target][:, 0, :])
         key_lane = lax.broadcasted_iota(jnp.int32, (SEL, rows), 1)

time: 22.4 us -> 22.4 us (level)
  the two profiles are of different devices: /device:TPU:11 before, /device:TPU:31 now
where the time goes in v5:
time: 22.4 us; the launch traced here: 22.2 us
  Pallas kernels  20.3 us (91%)
  local copies, waits for them, and re-layouts  1.87 us (8%)
    pallas_call x1, Pallas kernels, local(): pl.pallas_call(functools.partial(kernel, spans), out_shape=jax.ShapeDtype...  20.3 us
    unnamed x1, local copies, waits for them, and re-layouts  1.87 us

profile of v5, /device:TPU:31, one launch (start us, length us, event | category | flops | bytes accessed | tf_op | source)
XLA Modules:
  0.0 22.2 jit_solution(16230919673822398741)
XLA Ops:
  0.0 20.3 %shard_map.136 = bf16[512,512]{1,0:T(8,128)(2,1)} custom-call(bf16[512,1024]{1,0:T(8,128)(2,1)} %tokens_h.1, s32[8,1,16]{2,1,0:T(1,128)} %chosen_ref.1, bf16[1024,256]{1,0:T(8,128)(2,1)} %wq_h.1, bf16[1024,128]{1,0:T(8,128)(2,1)} %wks_h.1, bf16[1024,128]{1,0:T(8,128)(2,1)} %wvs_h.1, bf16[1024,128]{1,0:T(8,128)(2,1)} %wkc_h.1, bf16[1024,128]{1,0:T(8,128)(2,1)} %wvc_h.1, ...), custom_call_target="tpu_custom_call" | custom-call | tf_op jit(solution)/shard_map/pallas_call | solution.py:494
  20.3 1.9 %copy.16 = bf16[512,512]{1,0:T(8,128)(2,1)} copy(bf16[512,512]{1,0:T(8,128)(2,1)} %shard_map.136) | data formatting | bytes 1048576
